TPU v7x, 256 devices: a whole 4x4x8 slice. The times are simulated.
256 devices in a mesh: ep: 64 (over z, x, core), tp: 4 (over y).
Axes of the slice: x: 4, y: 4, z: 8, core: 2. Of those that a mesh axis runs over, the one named last changes fastest.
Arguments:
- query_rows: bfloat16 [12288, 1024], P('ep', 'tp'), may hold values from -8 to 8
- key_rows: bfloat16 [12288, 1024], P('ep', 'tp'), may hold values from -8 to 8
- value_rows: bfloat16 [12288, 1024], P('ep', 'tp'), may hold values from -6 to 6
- lambdas: float32 [8], P('tp'), may hold values from 0.3 to 0.8
- head_gain: float32 [128], replicated, may hold values from 0.1 to 1.9
- w_out: bfloat16 [1024, 2048], replicated, may hold values from -0.1875 to 0.1875
- moe_rows: bfloat16 [32768, 2048], P('ep'), may hold values from -6 to 6
- ffn_gain: float32 [2048], replicated, may hold values from 0.1 to 1.9
- routes: int32 [32768, 2], P('ep'), may hold values from 0 to 63, all different within a row; in each aligned block of 128 rows (0 to 127, 128 to 255, ...) at most 8 rows name the same one
- group_logits: float32 [32768, 4], P('ep'), may hold values from -8 to 8
- pick_logits: float32 [32768, 2], P('ep'), may hold values from -8 to 8
- w_gate: bfloat16 [64, 2048, 1024], P('ep', None, 'tp'), may hold values from -0.125 to 0.125
- w_up: bfloat16 [64, 2048, 1024], P('ep', None, 'tp'), may hold values from -0.125 to 0.125
- w_down: bfloat16 [64, 1024, 2048], P('ep', 'tp'), may hold values from -0.75 to 0.75
Outputs:
- mixer_out: bfloat16 [12288, 2048], P(('ep', 'tp'))
- moe_out: bfloat16 [32768, 2048], P(('ep', 'tp'))
Inputs may be any that keep to these rules, and one draw needn't show every extreme that they name: `routes`: each row names 2 different experts. In each aligned block of 128 rows (the rows of one device) no expert is named by more than 8 rows; some expert is named by exactly 8 rows of a block.
All inputs are finite; a program needn't handle non-finite values.
Results may differ from a plain program's by a relative error of at most 0.015.
Values may be sent and summed in bfloat16 or wider, within the bound.
A program may use at most 128 MiB of HBM per device.

v0:
```python
import jax
import jax.numpy as jnp
from jax import lax
from jax.sharding import PartitionSpec as P

EPS = 1e-06
HEAD_SCALE = 0.8


def cut_along(x, dim, peers):
    before, after = (x.shape[:dim], x.shape[dim + 1 :])
    return jnp.moveaxis(x.reshape(*before, peers, -1, *after), dim, 0)


def sent_and_summed(x, axis, dim):
    peers = lax.axis_size(axis)
    blocks = lax.all_to_all(cut_along(x, dim, peers), axis, 0, 0, tiled=True)
    return jnp.sum(blocks.astype(jnp.float32), axis=0)


def laid_out(blocks, dim):
    blocks = jnp.moveaxis(blocks, 0, dim)
    dims = blocks.shape
    return blocks.reshape(*dims[:dim], dims[dim] * dims[dim + 1], *dims[dim + 2 :])


def copy_for_each(x, axis):
    peers = lax.axis_size(axis)
    return lax.all_to_all(jnp.broadcast_to(x[None], (peers, *x.shape)), axis, 0, 0, tiled=True)


def gather_directly(x, axis, dim):
    return laid_out(copy_for_each(x, axis), dim)


def rms_rows(values, gain):
    squared = jnp.mean(values * values, axis=-1, keepdims=True)
    return values * lax.rsqrt(squared + EPS) * gain


def slot_index(picks, expert_count, capacity):
    flattened = picks.reshape(picks.shape[0], -1)
    onehot = (flattened[..., None] == jnp.arange(expert_count, dtype=jnp.int32)).astype(jnp.int32)
    before = jnp.cumsum(onehot, axis=1) - onehot
    ranking = jnp.sum(before * onehot, axis=-1)
    return flattened * capacity + ranking


def expert_hidden(arrived, gate_weight, up_weight):
    gate_part = jnp.dot(arrived, gate_weight, preferred_element_type=jnp.float32)
    up_part = jnp.dot(arrived, up_weight, preferred_element_type=jnp.float32)
    return (jax.nn.silu(gate_part) * up_part).astype(jnp.bfloat16)


def local(
    query_rows,
    key_rows,
    value_rows,
    lambdas,
    head_gain,
    w_out,
    moe_rows,
    ffn_gain,
    routes,
    group_logits,
    pick_logits,
    w_gate,
    w_up,
    w_down,
):
    token_count = query_rows.shape[0]
    local_heads = lambdas.shape[0]
    head_qk = query_rows.shape[1] // (2 * local_heads)
    head_v = value_rows.shape[1] // local_heads
    score_scale = head_qk ** (-0.5)
    queries = query_rows.reshape(token_count, local_heads, 2, head_qk)

    def absorb(carried, key_value):
        key_block, value_block = key_value
        running_max, running_sum, running_acc = carried
        scores = (
            jnp.einsum("qhmd,khmd->hmqk", queries, key_block, preferred_element_type=jnp.float32)
            * score_scale
        )
        new_max = jnp.maximum(running_max, jnp.max(scores, axis=-1))
        factor = jnp.exp(running_max - new_max)
        weights = jnp.exp(scores - new_max[..., None])
        running_sum = running_sum * factor + jnp.sum(weights, axis=-1)
        update = jnp.einsum(
            "hmqk,khv->hmqv",
            weights.astype(jnp.bfloat16),
            value_block,
            preferred_element_type=jnp.float32,
        )
        return ((new_max, running_sum, running_acc * factor[..., None] + update), None)

    start_state = (
        jnp.full((local_heads, 2, token_count), -1e30, jnp.float32),
        jnp.zeros((local_heads, 2, token_count), jnp.float32),
        jnp.zeros((local_heads, 2, token_count, head_v), jnp.float32),
    )
    carried = start_state
    key_piece = lax.all_gather(key_rows, "ep", axis=0, tiled=True)
    value_piece = lax.all_gather(value_rows, "ep", axis=0, tiled=True)
    length = key_piece.shape[0]
    block_rows = 1024
    blocks = (
        key_piece.reshape(length // block_rows, block_rows, local_heads, 2, head_qk),
        value_piece.reshape(length // block_rows, block_rows, local_heads, head_v),
    )
    carried, unused = lax.scan(absorb, carried, blocks)
    unused_max, final_sum, final_acc = carried
    averaged = final_acc / final_sum[..., None]
    per_head = averaged[:, 0] - lambdas[:, None, None] * averaged[:, 1]
    normed_heads = rms_rows(per_head, head_gain) * HEAD_SCALE
    attended = (
        jnp.transpose(normed_heads, (1, 0, 2))
        .reshape(token_count, local_heads * head_v)
        .astype(jnp.bfloat16)
    )
    own_weight = lax.dynamic_slice_in_dim(
        w_out, lax.axis_index("tp") * attended.shape[1], attended.shape[1], 0
    )
    mixer_out = sent_and_summed(
        jnp.dot(attended, own_weight, preferred_element_type=jnp.float32).astype(jnp.bfloat16),
        "tp",
        0,
    ).astype(jnp.bfloat16)
    quarters = lax.axis_size("tp")
    own_quarter = lax.axis_index("tp")
    expert_count = lax.axis_size("ep")
    model_width = moe_rows.shape[1]
    quarter_rows = moe_rows.shape[0] // quarters
    top_k = routes.shape[1]
    capacity = max(2, 2 * top_k * quarter_rows // expert_count)
    source_rows = jnp.repeat(jnp.arange(quarter_rows, dtype=jnp.int32), top_k)
    own_picks = lax.dynamic_slice_in_dim(routes, own_quarter * quarter_rows, quarter_rows, 0)
    own_tokens = lax.dynamic_slice_in_dim(moe_rows, own_quarter * quarter_rows, quarter_rows, 0)
    normed = rms_rows(own_tokens.astype(jnp.float32), ffn_gain).astype(jnp.bfloat16)
    own_slots = slot_index(own_picks[None], expert_count, capacity)[0]
    outgoing = (
        jnp.zeros((expert_count * capacity, model_width), jnp.bfloat16)
        .at[own_slots]
        .set(normed[source_rows])
    )
    arrived = lax.all_to_all(
        outgoing.reshape(expert_count, capacity, model_width),
        "ep",
        split_axis=0,
        concat_axis=0,
        tiled=True,
    )
    pieces = gather_directly(arrived, "tp", 0)
    flat_rows = pieces.reshape(-1, model_width)
    hidden = expert_hidden(flat_rows, w_gate[0], w_up[0]).reshape(pieces.shape[0], capacity, -1)
    hidden_flat = hidden.reshape(-1, hidden.shape[-1])
    summed = lax.psum_scatter(
        jnp.dot(hidden_flat, w_down[0], preferred_element_type=jnp.float32).astype(jnp.bfloat16),
        "tp",
        scatter_dimension=0,
        tiled=True,
    )
    returned = lax.all_to_all(
        summed.reshape(expert_count, capacity, model_width),
        "ep",
        split_axis=0,
        concat_axis=0,
        tiled=True,
    )
    picked = returned.reshape(-1, model_width)[own_slots].reshape(quarter_rows, top_k, model_width)
    own_groups = lax.dynamic_slice_in_dim(group_logits, own_quarter * quarter_rows, quarter_rows, 0)
    own_pick_logits = lax.dynamic_slice_in_dim(
        pick_logits, own_quarter * quarter_rows, quarter_rows, 0
    )
    group_count = group_logits.shape[1]
    group_prob = jax.nn.softmax(own_groups, axis=-1)
    group_index = own_picks // (expert_count // group_count)
    matches = (group_index[..., None] == jnp.arange(group_count, dtype=jnp.int32)).astype(
        jnp.float32
    )
    group_share = jnp.sum(group_prob[:, None, :] * matches, axis=-1)
    gate_values = group_share * jax.nn.softmax(own_pick_logits, axis=-1)
    moe_out = jnp.sum(gate_values[..., None] * picked.astype(jnp.float32), axis=1).astype(
        jnp.bfloat16
    )
    return (mixer_out, moe_out)


def solution(mesh):
    return jax.shard_map(
        local,
        mesh=mesh,
        in_specs=(
            P("ep", "tp"),
            P("ep", "tp"),
            P("ep", "tp"),
            P("tp"),
            P(),
            P(),
            P("ep", None),
            P(),
            P("ep", None),
            P("ep", None),
            P("ep", None),
            P("ep", None, "tp"),
            P("ep", None, "tp"),
            P("ep", "tp", None),
        ),
        out_specs=(P(("ep", "tp"), None), P(("ep", "tp"), None)),
        check_vma=False,
    )
```

profile of v0, /device:TPU:1, one launch (start us, length us, event | category | flops | bytes accessed | tf_op | source)
XLA Modules:
  0.0 442.0 jit_solution(13916826065649422579)
XLA Ops:
  13.5 2.0 fusion.20
  15.5 6.2 %scatter_custom_fusion = bf16[512,2048]{1,0:T(8,128)(2,1)S(1)} fusion(s32[256]{0:T(256)S(1)} %bitcast.113, bf16[128,2048]{1,0:T(8,128)(2,1)} %fusion.20, s32[1024]{0:T(1024)S(1)} %pad_clamp_fusion.1, bf16[]{:T(256)} %constant.43.clone.1), kind=kCustom, calls=%fused_computation.39 | custom fusion | bytes 2097664 | tf_op jit(solution)/shard_map/scatter | solution.py:144
  21.7 70.8 %all_to_all.20 = bf16[64,8,2048]{2,1,0:T(8,128)(2,1)S(1)} all-to-all(bf16[64,8,2048]{2,1,0:T(8,128)(2,1)S(1)} %bitcast.104), channel_id=1, replica_groups=mesh['ep'=64,'tp'=4] {'ep'}, dimensions={0} | all-to-all | bytes 4194304 | tf_op jit(solution)/shard_map/all_to_all | solution.py:146
  92.5 4.3 broadcast_in_dim.19
  96.8 5.8 %all-to-all-start.2 = ((bf16[4,64,8,2048]{3,2,1,0:T(8,128)(2,1)}), bf16[4,64,8,2048]{3,2,1,0:T(8,128)(2,1)}, u32[]{:S(2)}, u32[]{:S(2)}) async-start(bf16[4,64,8,2048]{3,2,1,0:T(8,128)(2,1)} %broadcast_in_dim.19), calls=%async_computation.2 | async-start | bytes 16777216 | tf_op jit(solution)/shard_map/all_to_all | solution.py:29
  103.0 90.9 %all-to-all-done.2 = bf16[4,64,8,2048]{3,2,1,0:T(8,128)(2,1)} async-done(((bf16[4,64,8,2048]{3,2,1,0:T(8,128)(2,1)}), bf16[4,64,8,2048]{3,2,1,0:T(8,128)(2,1)}, u32[]{:S(2)}, u32[]{:S(2)}) %all-to-all-start.2) | async-done | bytes 8388640 | tf_op jit(solution)/shard_map/all_to_all | solution.py:29
  193.8 7.1 %fusion.24 = f32[2048,256]{1,0:T(8,128)} fusion(bf16[2048,2048]{1,0:T(8,128)(2,1)} %bitcast.15, bf16[1,2048,256]{2,1,0:T(8,128)(2,1)S(1)} %copy-done.9), kind=kOutput, calls=%fused_computation.37 | convolution fusion | flops 2147483648 | bytes 11534336 | tf_op jit(solution)/shard_map/dot_general | solution.py:50
  201.0 16.8 %convolution_convert_fusion = bf16[2048,2048]{1,0:T(8,128)(2,1)} fusion(bf16[2048,2048]{1,0:T(8,128)(2,1)} %bitcast.15, f32[2048,256]{1,0:T(8,128)} %fusion.24, bf16[1,256,2048]{2,1,0:T(8,128)(2,1)S(1)} %copy-done, bf16[1,2048,256]{2,1,0:T(8,128)(2,1)} %param.28), kind=kOutput, calls=%fused_computation.25 | convolution fusion | flops 4302307328 | bytes 20971520 | tf_op jit(solution)/shard_map/dot_general | solution.py:158
  217.8 21.8 %reshape.281 = bf16[12,1024,2,2,64]{4,3,2,1,0:T(2,128)(2,1)} reshape(bf16[12288,256]{1,0:T(8,128)(2,1)} %all-gather.3.cloned.1.call-done) | data formatting | bytes 12582912 | tf_op jit(solution)/shard_map/reshape | solution.py:108
  239.6 29.7 %copy.37 = bf16[12,1024,2,2,64]{1,4,3,2,0:T(8,128)(2,1)} copy(bf16[12,1024,2,2,64]{4,3,2,1,0:T(2,128)(2,1)} %reshape.281) | data formatting | bytes 12582912
  269.3 9.8 %reshape.244 = bf16[12,1024,2,128]{3,2,1,0:T(2,128)(2,1)} reshape(bf16[12288,256]{1,0:T(8,128)(2,1)} %all-gather.5.cloned.1.call-done) | data formatting | bytes 12582912 | tf_op jit(solution)/shard_map/reshape | solution.py:109
  279.1 67.7 %while.15 = (s32[]{:T(128)}, f32[2,2,192]{2,1,0:T(2,128)S(1)}, f32[2,2,192]{2,1,0:T(2,128)S(1)}, f32[2,2,192,128]{3,2,1,0:T(8,128)}, bf16[12,1024,2,2,64]{1,4,3,...) while((s32[]{:T(128)}, f32[2,2,192]{2,1,0:T(2,128)S(1)}, ...), condition=%wide.region_3.4_spmd.clone, body=%wide.region_0.3_spmd.clone.sunk | while | flops 308580096 | bytes 15614629 | solution.py:111
  279.1 1.8 bitcast_reduce_fusion.2
  290.4 1.7 bitcast_reduce_fusion.2
  301.7 1.7 bitcast_reduce_fusion.2
  307.4 1.7 bitcast_reduce_fusion.2
  313.0 1.7 bitcast_reduce_fusion.2
  324.3 1.7 bitcast_reduce_fusion.2
  350.0 11.1 %all_to_all.21 = bf16[4,48,2048]{2,1,0:T(8,128)(2,1)S(1)} all-to-all(bf16[4,48,2048]{2,1,0:T(8,128)(2,1)S(1)} %bitcast.106), channel_id=1, replica_groups=mesh['ep'=64,'tp'=4] {'tp'}, dimensions={0} | all-to-all | bytes 1572864 | tf_op jit(solution)/shard_map/all_to_all | solution.py:17
  361.1 15.1 %all-to-all-start.3 = ((bf16[64,8,2048]{2,1,0:T(8,128)(2,1)}), bf16[64,8,2048]{2,1,0:T(8,128)(2,1)S(1)}, u32[]{:S(2)}, u32[]{:S(2)}) async-start(bf16[64,8,2048]{2,1,0:T(8,128)(2,1)} %bitcast.107), calls=%async_computation.4 | async-start | bytes 4194304 | tf_op jit(solution)/shard_map/all_to_all | solution.py:163
  377.3 48.6 %all-to-all-done.3 = bf16[64,8,2048]{2,1,0:T(8,128)(2,1)S(1)} async-done(((bf16[64,8,2048]{2,1,0:T(8,128)(2,1)}), bf16[64,8,2048]{2,1,0:T(8,128)(2,1)S(1)}, u32[]{:S(2)}, u32[]{:S(2)}) %all-to-all-start.3) | async-done | bytes 2097184 | tf_op jit(solution)/shard_map/all_to_all | solution.py:163
  425.9 2.3 gather_fusion
  428.3 2.4 reshape.255
  430.6 3.9 multiply_reduce_fusion
  (191 shorter events, 66.5 us)
Async XLA Ops:
  8.0 193.0 %copy-start = (bf16[1,256,2048]{2,1,0:T(8,128)(2,1)S(1)}, bf16[1,256,2048]{2,1,0:T(8,128)(2,1)}, u32[]{:S(2)}) copy-start(bf16[1,256,2048]{2,1,0:T(8,128)(2,1)} %param.29) | copy-start | bytes 3145732
  8.0 209.7 %all-gather.3.cloned.1.call-start = ((), (), s32[]{:S(2)}) async-start(), calls=%async_computation.5 | async-start | bytes 6389760 | tf_op jit(solution)/shard_map/all_gather | solution.py:103
  8.7 260.6 %all-gather.5.cloned.1.call-start = ((), (), s32[]{:S(2)}) async-start(), calls=%async_computation.6 | async-start | bytes 6389760 | tf_op jit(solution)/shard_map/all_gather | solution.py:104
  96.8 6.1 %copy-start.4 = (bf16[192,256]{1,0:T(8,128)(2,1)S(1)}, bf16[192,256]{1,0:T(8,128)(2,1)}, u32[]{:S(2)}) copy-start(bf16[192,256]{1,0:T(8,128)(2,1)} %param.16) | copy-start | bytes 294916
  96.8 97.1 %copy-start.9 = (bf16[1,2048,256]{2,1,0:T(8,128)(2,1)S(1)}, bf16[1,2048,256]{2,1,0:T(8,128)(2,1)}, u32[]{:S(2)}) copy-start(bf16[1,2048,256]{2,1,0:T(8,128)(2,1)} %param.27) | copy-start | bytes 3145732
  96.8 97.0 %all-to-all-start.2 = ((bf16[4,64,8,2048]{3,2,1,0:T(8,128)(2,1)}), bf16[4,64,8,2048]{3,2,1,0:T(8,128)(2,1)}, u32[]{:S(2)}, u32[]{:S(2)}) async-start(bf16[4,64,8,2048]{3,2,1,0:T(8,128)(2,1)} %broadcast_in_dim.19), calls=%async_computation.2 | async-start | bytes 16777216 | tf_op jit(solution)/shard_map/all_to_all | solution.py:29
  102.6 258.5 %reduce-scatter.2.cloned.1.call-start = ((), (), s32[]{:S(2)}) async-start(), calls=%async_computation.7 | async-start | bytes 10485760 | tf_op jit(solution)/shard_map/reduce_scatter | solution.py:157
  279.1 68.9 %copy-start.7 = (f32[2]{0:T(128)S(1)}, f32[2]{0:T(128)}, u32[]{:S(2)}) copy-start(f32[2]{0:T(128)} %param.19) | copy-start | bytes 28
  279.1 69.2 %copy-start.8 = (f32[128]{0:T(128)S(1)}, f32[128]{0:T(128)}, u32[]{:S(2)}) copy-start(f32[128]{0:T(128)} %param.20) | copy-start | bytes 1540
  280.9 2.2 copy-start.2
  286.5 2.2 copy-start.2
  292.2 2.2 copy-start.2
  297.8 2.2 copy-start.2
  303.5 2.2 copy-start.2
  309.1 2.2 copy-start.2
  314.8 2.2 copy-start.2
  320.4 2.2 copy-start.2
  326.0 2.2 copy-start.2
  337.3 2.2 copy-start.2
  343.0 2.2 copy-start.2
  350.0 26.3 %copy-start.5 = (f32[512,4]{0,1:T(4,128)S(1)}, f32[512,4]{0,1:T(4,128)}, u32[]{:S(2)}) copy-start(f32[512,4]{0,1:T(4,128)} %param.25) | copy-start | bytes 24580
  350.0 26.3 %copy-start.6 = (f32[512,2]{0,1:T(2,128)S(1)}, f32[512,2]{0,1:T(2,128)}, u32[]{:S(2)}) copy-start(f32[512,2]{0,1:T(2,128)} %param.26) | copy-start | bytes 12292
  361.1 64.8 %all-to-all-start.3 = ((bf16[64,8,2048]{2,1,0:T(8,128)(2,1)}), bf16[64,8,2048]{2,1,0:T(8,128)(2,1)S(1)}, u32[]{:S(2)}, u32[]{:S(2)}) async-start(bf16[64,8,2048]{2,1,0:T(8,128)(2,1)} %bitcast.107), calls=%async_computation.4 | async-start | bytes 4194304 | tf_op jit(solution)/shard_map/all_to_all | solution.py:163
  425.9 8.7 %copy-start.1 = (bf16[1,256,2048]{2,1,0:T(8,128)(2,1)S(1)}, bf16[1,256,2048]{2,1,0:T(8,128)(2,1)}, u32[]{:S(2)}) copy-start(bf16[1,256,2048]{2,1,0:T(8,128)(2,1)} %param.29) | copy-start | bytes 3145732
  (13 other events, 11.1 us)
Sparse Core Ops, SparseCore 0:
  11.6 96.1 all-gather.2
  110.6 78.3 all-gather.4
Sparse Core Ops, SparseCore 1:
  217.8 83.4 reduce-scatter.1
where the time goes:
time: 445 us; the launch traced here: 442 us
  waiting for transfers between devices  141 us (32%)
  local copies, waits for them, and re-layouts  104 us (23%)
  blocking collectives  81.9 us (18%)
  matrix products  58.1 us (13%)
  starting transfers between devices  21.2 us (5%)
  other arithmetic  19.7 us (4%)
  between operations  15.7 us (4%)
    all_to_all x1, waiting for transfers between devices, copy_for_each(): lax.all_to_all(jnp.broadcast_to(x[None], (peers, *x.shape)), axis, 0, 0,...  90.9 us
    all_to_all x1, blocking collectives, local(): lax.all_to_all(outgoing.reshape(expert_count, capacity, model_width), 'ep...  70.8 us
    all_to_all x1, waiting for transfers between devices, local(): lax.all_to_all(summed.reshape(expert_count, capacity, model_width), 'ep',...  48.6 us
    unnamed x18, local copies, waits for them, and re-layouts  29.9 us
    reshape x1, local copies, waits for them, and re-layouts, local(): key_piece.reshape(length // block_rows, block_rows, local_heads, 2, head_qk)  21.8 us
    dot_general x12, matrix products, absorb(): jnp.einsum('qhmd,khmd->hmqk', queries, key_block, preferred_element_type=...  20.9 us
    dynamic_slice x12, local copies, waits for them, and re-layouts, local(): carried, unused = lax.scan(absorb, carried, blocks)  16.9 us
    dot_general x1, matrix products, local(): jnp.dot(hidden_flat, w_down[0], preferred_element_type=jnp.float32)  16.8 us
  transfers between devices with their start and end apart: 5, of which 2 were waited for; matrix products, arithmetic and copies ran while one was open for 37% of the time, Pallas kernels for 0%

commit v1 on v0

v1 whole, which is shorter than its diff:
```python
import functools

import jax
import jax.numpy as jnp
from jax import lax
from jax.experimental import pallas as pl
from jax.experimental.pallas import tpu as pltpu
from jax.sharding import PartitionSpec as P

EPS = 1e-06
HEAD_SCALE = 0.8
NZ, NX, NC, NY = 8, 4, 2, 4
ANY = pl.BlockSpec(memory_space=pl.ANY)
VMEM = pl.BlockSpec(memory_space=pltpu.VMEM)
MESH = pl.DeviceIdType.MESH


def rms_rows(values, gain):
    squared = jnp.mean(values * values, axis=-1, keepdims=True)
    return values * lax.rsqrt(squared + EPS) * gain


def plane_peer(ep, i):
    z, x, c = ep // (NX * NC), ep // NC % NX, ep % NC
    k, j = i % NZ, i // NZ
    dz = lax.rem(jnp.where(k % 2 == 1, (k + 1) // 2, NZ - k // 2), NZ)
    dx, dc = j // NC, j % NC
    return (lax.rem(z + dz, NZ) * NX + lax.rem(x + dx, NX)) * NC + lax.rem(c + dc, NC)


def gather_kernel(
    out_ref, g_ref, u_ref, d_ref, arrived_ref, gs_ref, us_ref, ds_ref, a_send, a_recv, w_send, w_recv, own_sem
):
    ep, tp = lax.axis_index("ep"), lax.axis_index("tp")
    right, left = lax.rem(tp + 1, NY), lax.rem(tp + NY - 1, NY)
    weights = ((g_ref, gs_ref), (u_ref, us_ref), (d_ref, ds_ref))

    def half(ref, h):
        rows = ref.shape[-2] // 2
        return ref.at[pl.ds(h * rows, rows)]

    def first(n, h, to_right):
        src, dst = weights[n]
        slot = 0 if to_right else 1
        at = (slot * 3 + n) * 2 + h
        return pltpu.make_async_remote_copy(
            src_ref=half(src, h),
            dst_ref=half(dst.at[slot], h),
            send_sem=w_send.at[at],
            recv_sem=w_recv.at[at],
            device_id=(ep, right if to_right else left),
            device_id_type=MESH,
        )

    def onward(n, to_right):
        src, dst = weights[n]
        slot, h = (0, 0) if to_right else (1, 1)
        at = 12 + slot * 3 + n
        return pltpu.make_async_remote_copy(
            src_ref=half(dst.at[slot], h),
            dst_ref=half(dst.at[2], h),
            send_sem=w_send.at[at],
            recv_sem=w_recv.at[at],
            device_id=(ep, right if to_right else left),
            device_id_type=MESH,
        )

    for turn in range(2):
        for n in range(3):
            first(n, turn, True).start()
            first(n, 1 - turn, False).start()

    def dispatch(i):
        peer = plane_peer(ep, i)
        return pltpu.make_async_remote_copy(
            src_ref=out_ref.at[peer],
            dst_ref=arrived_ref.at[ep],
            send_sem=a_send.at[i],
            recv_sem=a_recv.at[i],
            device_id=(peer, tp),
            device_id_type=MESH,
        )

    own = pltpu.make_async_copy(out_ref.at[ep], arrived_ref.at[ep], own_sem)
    own.start()

    def begin(i, carry):
        dispatch(i).start()
        return carry

    lax.fori_loop(1, NZ * NX * NC, begin, 0)
    for n in range(3):
        first(n, 0, True).wait_recv()
        onward(n, True).start()
        first(n, 1, False).wait_recv()
        onward(n, False).start()
    own.wait()

    def finish(i, carry):
        dispatch(i).wait()
        return carry

    lax.fori_loop(1, NZ * NX * NC, finish, 0)
    for n in range(3):
        first(n, 1, True).wait_recv()
        first(n, 0, False).wait_recv()
        for to_right in (True, False):
            first(n, 0, to_right).wait_send()
            first(n, 1, to_right).wait_send()
            onward(n, to_right).wait()


def gather_all(outgoing, w_gate, w_up, w_down):
    shape = lambda w: jax.ShapeDtypeStruct((3, *w.shape), w.dtype)
    peers = NZ * NX * NC
    return pl.pallas_call(
        gather_kernel,
        name="gather_all",
        out_shape=(jax.ShapeDtypeStruct(outgoing.shape, outgoing.dtype), shape(w_gate), shape(w_up), shape(w_down)),
        in_specs=[ANY] * 4,
        out_specs=(ANY,) * 4,
        scratch_shapes=[
            pltpu.SemaphoreType.DMA((peers,)),
            pltpu.SemaphoreType.DMA((peers,)),
            pltpu.SemaphoreType.DMA((18,)),
            pltpu.SemaphoreType.DMA((18,)),
            pltpu.SemaphoreType.DMA,
        ],
        compiler_params=pltpu.CompilerParams(has_side_effects=True),
        cost_estimate=pl.CostEstimate(flops=10**11, bytes_accessed=30 * 2**20, transcendentals=0),
    )(outgoing, w_gate, w_up, w_down)


def experts_kernel(x_ref, g_ref, u_ref, d_ref, gs_ref, us_ref, ds_ref, out_ref, total):
    def add(gate_weight, up_weight, down_weight, start):
        x = x_ref[...]
        gate = jnp.dot(x, gate_weight, preferred_element_type=jnp.float32)
        up = jnp.dot(x, up_weight, preferred_element_type=jnp.float32)
        hidden = (gate / (1.0 + jnp.exp(-gate)) * up).astype(jnp.bfloat16)
        part = jnp.dot(hidden, down_weight, preferred_element_type=jnp.float32)
        if start:
            total[...] = part
        else:
            total[...] += part

    step = pl.program_id(0)

    @pl.when(step == 0)
    def _():
        add(g_ref[...], u_ref[...], d_ref[...], True)

    @pl.when(step > 0)
    def _():
        add(gs_ref[0], us_ref[0], ds_ref[0], False)

    @pl.when(step == NY - 1)
    def _():
        out_ref[...] = total[...].astype(jnp.bfloat16)


def experts(rows, w_gate, w_up, w_down, gates, ups, downs):
    other = lambda w: pl.BlockSpec((1, *w.shape[1:]), lambda i: (jnp.maximum(i - 1, 0), 0, 0))
    whole = lambda w: pl.BlockSpec(w.shape, lambda i: (0, 0))
    return pl.pallas_call(
        experts_kernel,
        name="experts",
        grid=(NY,),
        out_shape=jax.ShapeDtypeStruct(rows.shape, jnp.bfloat16),
        in_specs=[whole(rows), whole(w_gate), whole(w_up), whole(w_down), other(gates), other(ups), other(downs)],
        out_specs=whole(rows),
        scratch_shapes=[pltpu.VMEM(rows.shape, jnp.float32)],
        compiler_params=pltpu.CompilerParams(
            dimension_semantics=("arbitrary",), vmem_limit_bytes=48 * 2**20
        ),
        cost_estimate=pl.CostEstimate(flops=6 * 10**9, bytes_accessed=16 * 2**20, transcendentals=0),
    )(rows, w_gate, w_up, w_down, gates, ups, downs)


def return_kernel(
    block,
    rows_ref, q_ref, kv_ref, lam_ref, gain_ref, returned_ref, heads_ref,
    kv, top, total, acc, done, a_send, a_recv, h_send, h_recv, own_sem,
):
    ep, tp = lax.axis_index("ep"), lax.axis_index("tp")
    chip, core = ep // NC, ep % NC
    head = tp * NC + core

    def give_back(i):
        peer = plane_peer(ep, i)
        return pltpu.make_async_remote_copy(
            src_ref=rows_ref.at[peer],
            dst_ref=returned_ref.at[ep],
            send_sem=a_send.at[i],
            recv_sem=a_recv.at[i],
            device_id=(peer, tp),
            device_id_type=MESH,
        )

    own = pltpu.make_async_copy(rows_ref.at[ep], returned_ref.at[ep], own_sem.at[0])
    load = pltpu.make_async_copy(kv_ref, kv, own_sem.at[1])
    own.start()
    load.start()

    def begin(i, carry):
        give_back(i).start()
        return carry

    lax.fori_loop(1, NZ * NX * NC, begin, 0)
    top[...] = jnp.full_like(top, -1e30)
    total[...] = jnp.zeros_like(total)
    acc[...] = jnp.zeros_like(acc)
    load.wait()

    def absorb(b, carry):
        rows = pl.ds(pl.multiple_of(b * block, block), block)
        keys = kv[rows, 0:128]
        scores = lax.dot_general(
            q_ref[...], keys, (((1,), (1,)), ((), ())), preferred_element_type=jnp.float32
        )
        old = top[...]
        new = jnp.maximum(old, jnp.max(scores, axis=-1, keepdims=True))
        factor = jnp.exp(old - new)
        weights = jnp.exp(scores - new)
        total[...] = total[...] * factor + jnp.sum(weights, axis=-1, keepdims=True)
        acc[...] = acc[...] * factor + jnp.dot(
            weights.astype(jnp.bfloat16), kv[rows, 128:256], preferred_element_type=jnp.float32
        )
        top[...] = new
        return carry

    lax.fori_loop(0, kv.shape[0] // block, absorb, 0)
    count = acc.shape[0] // 2
    per_head = acc[0:count] / total[0:count] - lam_ref[...] * (acc[count:] / total[count:])
    squared = jnp.mean(per_head * per_head, axis=-1, keepdims=True)
    normed = per_head * lax.rsqrt(squared + EPS) * gain_ref[...] * HEAD_SCALE
    done[...] = normed.astype(jnp.bfloat16).reshape(done.shape)

    def hand_on(i):
        to_core = lax.rem(core + i // NY, NC)
        to_tp = lax.rem(tp + i % NY, NY)
        return pltpu.make_async_remote_copy(
            src_ref=done.at[to_core * NY + to_tp],
            dst_ref=heads_ref.at[head],
            send_sem=h_send.at[i],
            recv_sem=h_recv.at[i],
            device_id=(chip * NC + to_core, to_tp),
            device_id_type=MESH,
        )

    keep = pltpu.make_async_copy(done.at[core * NY + tp], heads_ref.at[head], own_sem.at[2])
    keep.start()
    for i in range(1, NC * NY):
        hand_on(i).start()
    for i in range(1, NC * NY):
        hand_on(i).wait()
    keep.wait()
    own.wait()

    def finish(i, carry):
        give_back(i).wait()
        return carry

    lax.fori_loop(1, NZ * NX * NC, finish, 0)


def return_and_attend(rows, queries, keys_values, lam, gain):
    peers = NZ * NX * NC
    count = queries.shape[0]
    own_rows = count // 2 // (NC * NY)
    return pl.pallas_call(
        functools.partial(return_kernel, 1024),
        name="return_and_attend",
        out_shape=(
            jax.ShapeDtypeStruct(rows.shape, rows.dtype),
            jax.ShapeDtypeStruct((NC * NY, own_rows, 128), jnp.bfloat16),
        ),
        in_specs=[ANY, VMEM, ANY, VMEM, VMEM],
        out_specs=(ANY, ANY),
        scratch_shapes=[
            pltpu.VMEM(keys_values.shape, jnp.bfloat16),
            pltpu.VMEM((count, 1), jnp.float32),
            pltpu.VMEM((count, 1), jnp.float32),
            pltpu.VMEM((count, 128), jnp.float32),
            pltpu.VMEM((NC * NY, own_rows, 128), jnp.bfloat16),
            pltpu.SemaphoreType.DMA((peers,)),
            pltpu.SemaphoreType.DMA((peers,)),
            pltpu.SemaphoreType.DMA((NC * NY,)),
            pltpu.SemaphoreType.DMA((NC * NY,)),
            pltpu.SemaphoreType.DMA((3,)),
        ],
        compiler_params=pltpu.CompilerParams(has_side_effects=True, vmem_limit_bytes=56 * 2**20),
        cost_estimate=pl.CostEstimate(flops=4 * 10**9, bytes_accessed=16 * 2**20, transcendentals=0),
    )(rows, queries, keys_values, lam, gain)


def local(
    query_rows, key_rows, value_rows, lambdas, head_gain, w_out, moe_rows, ffn_gain,
    routes, group_logits, pick_logits, w_gate, w_up, w_down,
):
    ep, tp = lax.axis_index("ep"), lax.axis_index("tp")
    core = ep % NC
    peers = NZ * NX * NC

    rows_in = jnp.stack([query_rows, key_rows, value_rows])
    mine = lax.dynamic_slice_in_dim(rows_in, core * 128, 128, 2)
    other = lax.dynamic_slice_in_dim(rows_in, (1 - core) * 128, 128, 2)
    theirs = lax.ppermute(other, "ep", [(i, i ^ 1) for i in range(peers)])
    pair = jnp.where(core == 0, jnp.concatenate([mine, theirs], 1), jnp.concatenate([theirs, mine], 1))
    groups = [[i for i in range(peers) if i % NC == c] for c in range(NC)]
    keys_values = lax.all_gather(
        jnp.concatenate([pair[1], pair[2]], axis=1), "ep", axis=0, tiled=True, axis_index_groups=groups
    )
    scaled = pair[0] * jnp.bfloat16(0.125)
    zero = jnp.zeros((scaled.shape[0], 64), jnp.bfloat16)
    queries = jnp.concatenate(
        [jnp.concatenate([scaled[:, :64], zero], 1), jnp.concatenate([zero, scaled[:, 64:]], 1)], 0
    )

    quarter = moe_rows.shape[0] // NY
    top_k = routes.shape[1]
    capacity = 8
    own = lambda a: lax.dynamic_slice_in_dim(a, tp * quarter, quarter, 0)
    picks = own(routes)
    normed = rms_rows(own(moe_rows).astype(jnp.float32), ffn_gain).astype(jnp.bfloat16)
    flat = picks.reshape(-1)
    onehot = (flat[:, None] == jnp.arange(peers, dtype=jnp.int32)).astype(jnp.int32)
    ranking = jnp.sum((jnp.cumsum(onehot, axis=0) - onehot) * onehot, axis=-1)
    slots = (flat * capacity + ranking).reshape(quarter, top_k)
    at = slots[:, :, None] == jnp.arange(peers * capacity, dtype=jnp.int32)
    place = (at[:, 0] | at[:, 1]).astype(jnp.bfloat16)
    outgoing = lax.dot_general(
        place, normed, (((0,), (0,)), ((), ())), preferred_element_type=jnp.float32
    ).astype(jnp.bfloat16)

    arrived, gates, ups, downs = gather_all(
        outgoing.reshape(peers, capacity, -1), w_gate[0], w_up[0], w_down[0]
    )
    results = experts(arrived.reshape(peers * capacity, -1), w_gate[0], w_up[0], w_down[0], gates, ups, downs)
    returned, heads = return_and_attend(
        results.reshape(peers, capacity, -1),
        queries,
        keys_values,
        lax.dynamic_slice_in_dim(lambdas, core, 1, 0)[None],
        head_gain[None],
    )
    attended = jnp.transpose(heads, (1, 0, 2)).reshape(heads.shape[1], -1)
    mixer_out = jnp.dot(attended, w_out, preferred_element_type=jnp.float32).astype(jnp.bfloat16)

    group_count = group_logits.shape[1]
    group_prob = jax.nn.softmax(own(group_logits), axis=-1)
    matches = ((picks // (peers // group_count))[..., None] == jnp.arange(group_count, dtype=jnp.int32)).astype(
        jnp.float32
    )
    share = jnp.sum(group_prob[:, None, :] * matches, axis=-1)
    gate_values = share * jax.nn.softmax(own(pick_logits), axis=-1)
    mixing = jnp.sum(jnp.where(at, gate_values[:, :, None], 0.0), axis=1)
    high = mixing.astype(jnp.bfloat16)
    low = (mixing - high.astype(jnp.float32)).astype(jnp.bfloat16)
    back = returned.reshape(peers * capacity, -1)
    moe_out = (
        jnp.dot(high, back, preferred_element_type=jnp.float32)
        + jnp.dot(low, back, preferred_element_type=jnp.float32)
    ).astype(jnp.bfloat16)
    return mixer_out, moe_out


def solution(mesh):
    return jax.shard_map(
        local,
        mesh=mesh,
        in_specs=(
            P("ep", "tp"), P("ep", "tp"), P("ep", "tp"), P("tp"), P(), P(), P("ep", None), P(), P("ep", None),
            P("ep", None), P("ep", None), P("ep", None, "tp"), P("ep", None, "tp"), P("ep", "tp", None),
        ),
        out_specs=(P(("ep", "tp"), None), P(("ep", "tp"), None)),
        check_vma=False,
    )
```

time: 445 us -> 228 us (0.51)
  Pallas kernels: 0 us -> 194 us
  waiting for transfers between devices: 141 us -> 0.14 us
  local copies, waits for them, and re-layouts: 104 us -> 3.82 us
  blocking collectives: 81.9 us -> 0 us
  matrix products: 58.1 us -> 7.11 us
  starting transfers between devices: 21.2 us -> 3.32 us
  other arithmetic: 19.7 us -> 5.11 us
    pallas_call x0 -> x3, Pallas kernels: none -> 194 us  [the longest x1 117 us: gather_all(): pl.pallas_call(gather_kernel, name='gather_all', out_shape=(jax.ShapeDtyp...]
    all_to_all x2 -> x0, waiting for transfers between devices: 139 us -> none  [the longest x1 90.9 us: copy_for_each(): lax.all_to_all(jnp.broadcast_to(x[None], (peers, *x.shape)), axis, 0, 0,...]
    all_to_all x2 -> x0, blocking collectives: 81.9 us -> none  [the longest x1 70.8 us: local(): lax.all_to_all(outgoing.reshape(expert_count, capacity, model_width), 'ep...]
    dot_general x27 -> x4, matrix products: 58.1 us -> 7.11 us  [the longest x1 2.18 us: local(): jnp.dot(high, back, preferred_element_type=jnp.float32)]
    reshape x4 -> x0, local copies, waits for them, and re-layouts: 31.7 us -> none  [the longest x1 21.8 us: local(): key_piece.reshape(length // block_rows, block_rows, local_heads, 2, head_qk)]
    unnamed x18 -> x31, local copies, waits for them, and re-layouts: 29.9 us -> 2.32 us
    all_to_all x2 -> x0, starting transfers between devices: 20.9 us -> none  [the longest x1 15.1 us: local(): lax.all_to_all(summed.reshape(expert_count, capacity, model_width), 'ep',...]
    dynamic_slice x13 -> x3, local copies, waits for them, and re-layouts: 17 us -> 0.67 us  [the longest x1 0.61 us: local(): lax.dynamic_slice_in_dim(lambdas, core, 1, 0)[None]]
  transfers between devices with their start and end apart: 5 -> 2, of which waited for: 2 -> 1; matrix products, arithmetic and copies ran while one was open for 37% -> 3% of each run, Pallas kernels for 0% -> 56%
where the time goes in v1:
time: 228 us
  Pallas kernels  194 us (85%)
  between operations  14.4 us (6%)
  matrix products  7.11 us (3%)
  other arithmetic  5.11 us (2%)
  local copies, waits for them, and re-layouts  3.82 us (2%)
  starting transfers between devices  3.32 us (1%)
    pallas_call x1, Pallas kernels, gather_all(): pl.pallas_call(gather_kernel, name='gather_all', out_shape=(jax.ShapeDtyp...  117 us
    pallas_call x1, Pallas kernels, return_and_attend(): pl.pallas_call(functools.partial(return_kernel, 1024), name='return_and_a...  67.1 us
    pallas_call x1, Pallas kernels, experts(): pl.pallas_call(experts_kernel, name='experts', grid=(NY,), out_shape=jax....  10.1 us
  transfers between devices with their start and end apart: 2, of which 1 were waited for; matrix products, arithmetic and copies ran while one was open for 3% of the time, Pallas kernels for 56%

profile of v1, /device:TPU:1, one launch (start us, length us, event | category | flops | bytes accessed | tf_op | source)
XLA Modules:
  0.0 228.2 jit_solution(3648470799367979769)
XLA Ops:
  7.3 1.2 pad_maximum_fusion
  8.5 3.3 %collective-permute-start = (bf16[3,192,128]{2,1,0:T(8,128)(2,1)S(1)}, bf16[3,192,128]{2,1,0:T(8,128)(2,1)S(1)}, u32[]{:S(2)}, u32[]{:S(2)}) collective-permute-start(bf16[3,192,128]{2,1,0:T(8,128)(2,1)S(1)} %get-tuple-element.18), channel_id=1, source_target_pairs={{0,4},{4,0},{8,12},{12,8},{16,20},{20,16},{24,28},{28,24},{32,36},... | collective-permute-start | bytes 442376 | tf_op jit(solution)/shard_map/ppermute | solution.py:307
  11.9 0.1 eq.60
  12.1 0.6 reduce-window.6
  12.7 0.1 collective-permute-done
  12.9 0.7 copy-done.7
  13.7 0.7 pad_maximum_fusion.1
  14.4 0.2 slice_reduce_fusion
  14.6 0.1 eq.56
  14.9 0.1 reduce_sum.57
  15.3 0.6 dynamic_slice.25
  15.9 0.2 fusion.5
  16.2 0.1 select_reduce_fusion
  16.4 0.1 iota_compare_fusion
  16.5 2.1 fusion.out_ref
  18.7 117.1 %gather_all.1 = (bf16[64,8,2048]{2,1,0:T(8,128)(2,1)}, bf16[3,2048,256]{2,1,0:T(8,128)(2,1)}, bf16[3,2048,256]{2,1,0:T(8,128)(2,1)}, bf16[3,256,2048]{2,1,0:T(8,128)(2,1)}) custom-call(bf16[64,8,2048]{2,1,0:T(8,128)(2,1)} %fusion.out_ref, bf16[2048,256]{1,0:T(8,128)(2,1)} %bitcast.56, bf16[2048,256]{1,0:T(8,128)(2,1)} %bitcast.58, bf16[256,2048]{1,0:T(8,128)(2,1)} %bitcast.60), custom_call_target="tpu_custom_call" | custom-call | flops 99999997952 | bytes 31457280 | tf_op jit(solution)/shard_map/gather_all/pallas_call | solution.py:116
  135.9 10.1 %experts.1 = bf16[512,2048]{1,0:T(8,128)(2,1)S(1)} custom-call(bf16[512,2048]{1,0:T(8,128)(2,1)} %bitcast.67, bf16[2048,256]{1,0:T(8,128)(2,1)S(1)} %bitcast.57, bf16[2048,256]{1,0:T(8,128)(2,1)S(1)} %bitcast.59, bf16[256,2048]{1,0:T(8,128)(2,1)S(1)} %bitcast.61, bf16[3,2048,256]{2,1,0:T(8,128)(2,1)} %get-tuple-element.9.gs_ref, ...), custom_call_target="tpu_custom_call" | custom-call | flops 6000000000 | bytes 16777216 | tf_op jit(solution)/shard_map/experts/pallas_call | solution.py:164
  146.0 1.3 copy-done.4
  147.5 0.9 broadcast_select_fusion
  148.4 0.8 fusion.16.q_ref
  149.2 67.1 %return_and_attend.1 = (bf16[64,8,2048]{2,1,0:T(8,128)(2,1)}, bf16[8,48,128]{2,1,0:T(8,128)(2,1)}) custom-call(bf16[64,8,2048]{2,1,0:T(8,128)(2,1)} %bitcast.62, bf16[768,128]{1,0:T(8,128)(2,1)} %fusion.16.q_ref, bf16[12288,256]{1,0:T(8,128)(2,1)} %all-gather.2.cloned.1.call-done.kv_ref, f32[1,1]{1,0:T(1,128)} %bitcast.14.lam_ref, f32[1,128]{1,0:T(1,128)} %bitcast.66), custom_call_target="tpu_custom_call" | custom-call | flops 4000000000 | bytes 16777216 | tf_op jit(solution)/shard_map/return_and_attend/pallas_call | solution.py:270
  216.3 2.2 fusion.3
  218.5 1.3 fusion.1
  219.8 1.5 convolution_convert_fusion.1
  (52 shorter events, 1.1 us)
Async XLA Ops:
  7.2 4.7 %copy-start = (s32[512,2]{0,1:T(2,128)S(1)}, s32[512,2]{0,1:T(2,128)}, u32[]{:S(2)}) copy-start(s32[512,2]{0,1:T(2,128)} %param.22) | copy-start | bytes 12292
  7.2 8.0 %copy-start.11 = (f32[512,4]{0,1:T(4,128)S(1)}, f32[512,4]{0,1:T(4,128)}, u32[]{:S(2)}) copy-start(f32[512,4]{0,1:T(4,128)} %param.23) | copy-start | bytes 24580
  7.2 8.1 %copy-start.12 = (f32[512,2]{0,1:T(2,128)S(1)}, f32[512,2]{0,1:T(2,128)}, u32[]{:S(2)}) copy-start(f32[512,2]{0,1:T(2,128)} %param.24) | copy-start | bytes 12292
  7.2 8.1 %copy-start.14 = (f32[2]{0:T(128)S(1)}, f32[2]{0:T(128)}, u32[]{:S(2)}) copy-start(f32[2]{0:T(128)} %param.17) | copy-start | bytes 28
  7.2 8.7 %copy-start.8 = (bf16[512,2048]{1,0:T(8,128)(2,1)S(1)}, bf16[512,2048]{1,0:T(8,128)(2,1)}, u32[]{:S(2)}) copy-start(bf16[512,2048]{1,0:T(8,128)(2,1)} %param.20) | copy-start | bytes 6291460
  7.2 142.0 %all-gather.2.cloned.1.call-start = ((), (), s32[]{:S(2)}) async-start(), calls=%async_computation | async-start | bytes 6488064 | tf_op jit(solution)/shard_map/all_gather | solution.py:310
  8.5 8.1 %copy-start.10 = (f32[2048]{0:T(1024)S(1)}, f32[2048]{0:T(1024)}, u32[]{:S(2)}) copy-start(f32[2048]{0:T(1024)} %param.21) | copy-start | bytes 24580
  8.5 4.3 %collective-permute-start = (bf16[3,192,128]{2,1,0:T(8,128)(2,1)S(1)}, bf16[3,192,128]{2,1,0:T(8,128)(2,1)S(1)}, u32[]{:S(2)}, u32[]{:S(2)}) collective-permute-start(bf16[3,192,128]{2,1,0:T(8,128)(2,1)S(1)} %get-tuple-element.18), channel_id=1, source_target_pairs={{0,4},{4,0},{8,12},{12,8},{16,20},{20,16},{24,28},{28,24},{32,36},... | collective-permute-start | bytes 442376 | tf_op jit(solution)/shard_map/ppermute | solution.py:307
  12.9 0.7 copy-start.7
  18.7 117.2 %copy-start.1 = (bf16[1,2048,256]{2,1,0:T(8,128)(2,1)S(1)}, bf16[1,2048,256]{2,1,0:T(8,128)(2,1)}, u32[]{:S(2)}) copy-start(bf16[1,2048,256]{2,1,0:T(8,128)(2,1)} %param.25) | copy-start | bytes 3145732
  18.7 117.2 %copy-start.2 = (bf16[1,2048,256]{2,1,0:T(8,128)(2,1)S(1)}, bf16[1,2048,256]{2,1,0:T(8,128)(2,1)}, u32[]{:S(2)}) copy-start(bf16[1,2048,256]{2,1,0:T(8,128)(2,1)} %param.26) | copy-start | bytes 3145732
  18.7 117.2 %copy-start.3 = (bf16[1,256,2048]{2,1,0:T(8,128)(2,1)S(1)}, bf16[1,256,2048]{2,1,0:T(8,128)(2,1)}, u32[]{:S(2)}) copy-start(bf16[1,256,2048]{2,1,0:T(8,128)(2,1)} %param.27) | copy-start | bytes 3145732
  135.9 11.6 %copy-start.13 = (pred[128]{0:T(512)(128)(4,1)S(1)}, pred[128]{0:T(512)(128)(4,1)}, u32[]{:S(2)}) copy-start(pred[128]{0:T(512)(128)(4,1)} %constant.55.clone.1) | copy-start | bytes 388
  146.0 1.3 copy-start.4
  216.3 2.2 copy-start.5
  216.3 3.5 %copy-start.6 = (bf16[1024,2048]{1,0:T(8,128)(2,1)S(1)}, bf16[1024,2048]{1,0:T(8,128)(2,1)}, u32[]{:S(2)}) copy-start(bf16[1024,2048]{1,0:T(8,128)(2,1)} %param.19) | copy-start | bytes 12582916
  218.5 1.4 copy-start.9
Sparse Core Ops, SparseCore 0:
  14.5 102.4 all-gather.1

commit v2 on v1

v2 whole, which is shorter than its diff:
```python
import functools

import jax
import jax.numpy as jnp
from jax import lax
from jax.experimental import pallas as pl
from jax.experimental.pallas import tpu as pltpu
from jax.sharding import PartitionSpec as P

EPS = 1e-06
HEAD_SCALE = 0.8
NZ, NX, NC, NY = 8, 4, 2, 4
ANY = pl.BlockSpec(memory_space=pl.ANY)
VMEM = pl.BlockSpec(memory_space=pltpu.VMEM)
MESH = pl.DeviceIdType.MESH


def plane_peer(ep, i):
    z, x, c = ep // (NX * NC), ep // NC % NX, ep % NC
    k, j = i % NZ, i // NZ
    dz = lax.rem(jnp.where(k % 2 == 1, (k + 1) // 2, NZ - k // 2), NZ)
    dx, dc = j // NC, j % NC
    return (lax.rem(z + dz, NZ) * NX + lax.rem(x + dx, NX)) * NC + lax.rem(c + dc, NC)


def step_kernel(
    parts, block,
    q_ref, k_ref, v_ref, lam_ref, gain_ref, w_out_ref, rows_ref, ffn_ref, place_ref, high_ref, low_ref,
    g_ref, u_ref, d_ref, mixer_ref, moe_ref,
    gates, ups, downs, sent, arrived, hidden, results, returned, queries, spread, kv, top, total, acc, done, heads, w_out,
    g_send, g_recv, d_send, d_recv, p_send, p_recv, z_send, z_recv, x_send, x_recv,
    a_send, a_recv, r_send, r_recv, h_send, h_recv, own_sem,
):
    ep, tp = lax.axis_index("ep"), lax.axis_index("tp")
    z, x, core = ep // (NX * NC), ep // NC % NX, ep % NC
    chip = ep // NC
    head = tp * NC + core
    peers = NZ * NX * NC
    f32 = jnp.float32

    def remote(src, dst, send, recv, at, device):
        return pltpu.make_async_remote_copy(
            src_ref=src, dst_ref=dst, send_sem=send.at[at], recv_sem=recv.at[at],
            device_id=device, device_id_type=MESH,
        )

    tp_side = (lax.rem(tp + 1, NY), lax.rem(tp + NY - 1, NY))

    def gate_up(n, step, side):
        src, full = ((g_ref, gates), (u_ref, ups))[n]
        rows = src.shape[0] // 2
        h = (step + side) % 2 if step < 2 else side
        part = pl.ds(h * rows, rows)
        frm = src.at[part] if step < 2 else full.at[1 + side, part]
        to = full.at[1 + side if step < 2 else 3, part]
        return remote(frm, to, g_send, g_recv, (n * 3 + step) * 2 + side, (ep, tp_side[side]))

    def down(j, step, side):
        cols = downs.shape[2]
        rows = d_ref.shape[0] // 2
        h = (step + side) % 2 if step < 2 else side
        row = lambda place: pl.ds((place * 2 + h) * rows, rows)
        if step < 2:
            frm = d_ref.at[pl.ds(h * rows, rows), pl.ds(j * cols, cols)]
            to = downs.at[j, row(1 + side)]
        else:
            frm = downs.at[j, row(1 + side)]
            to = downs.at[j, row(3)]
        return remote(frm, to, d_send, d_recv, (j * 3 + step) * 2 + side, (ep, tp_side[side]))

    both = lambda make: [make(0), make(1)]

    for step in range(2):
        for n in range(2):
            for c in both(lambda side: gate_up(n, step, side)):
                c.start()

    mine = pl.ds(pl.multiple_of(core * 128, 128), 128)
    other = pl.ds(pl.multiple_of((1 - core) * 128, 128), 128)
    count = q_ref.shape[0]
    place_of = pl.ds(pl.multiple_of(core * count, count), count)
    kv_rows = pl.ds(pl.multiple_of((chip * NC + core) * count, count), count)
    triples = (
        (q_ref, queries.at[place_of]),
        (k_ref, kv.at[kv_rows, pl.ds(0, 128)]),
        (v_ref, kv.at[kv_rows, pl.ds(128, 128)]),
    )
    partner = chip * NC + 1 - core
    swaps = [remote(src.at[:, other], dst, p_send, p_recv, n, (partner, tp)) for n, (src, dst) in enumerate(triples)]
    keeps = [pltpu.make_async_copy(src.at[:, mine], dst, own_sem.at[n]) for n, (src, dst) in enumerate(triples)]
    for c in swaps + keeps:
        c.start()
    deep = d_ref.shape[0]
    cols = downs.shape[2]
    loads = [
        pltpu.make_async_copy(g_ref, gates.at[0], own_sem.at[3]),
        pltpu.make_async_copy(u_ref, ups.at[0], own_sem.at[4]),
        pltpu.make_async_copy(w_out_ref, w_out, own_sem.at[5]),
    ] + [
        pltpu.make_async_copy(d_ref.at[:, pl.ds(j * cols, cols)], downs.at[j, pl.ds(0, deep)], own_sem.at[6 + j])
        for j in range(parts)
    ]
    for c in loads:
        c.start()

    chip_rows = kv.shape[0] // (NZ * NX)
    at_z = lambda dz: lax.rem(z + dz + NZ, NZ)
    at_x = lambda dx: lax.rem(x + dx + NX, NX)

    def kv_block(dz, dx, h=None):
        start = (at_z(dz) * NX + at_x(dx)) * chip_rows
        rows = chip_rows
        if h is not None:
            rows = chip_rows // 2
            start = start + h * rows
        return kv.at[pl.ds(pl.multiple_of(start, rows), rows)]

    def along_z(hop, side):
        sign = 1 if side == 0 else -1
        ref = kv_block(-sign * (hop - 1), 0, side if hop == NZ // 2 else None)
        device = ((at_z(sign) * NX + x) * NC + core, tp)
        return remote(ref, ref, z_send, z_recv, (hop - 1) * 2 + side, device)

    blocks = [0, -1, 1, -2, 2, -3, 3, 4]

    def along_x(b, step, side):
        sign = 1 if side == 0 else -1
        ref = kv_block(blocks[b], 0) if step == 0 else kv_block(blocks[b], -sign, side)
        device = ((z * NX + at_x(sign)) * NC + core, tp)
        return remote(ref, ref, x_send, x_recv, (b * 2 + step) * 2 + side, device)

    def x_first(b):
        for c in both(lambda side: along_x(b, 0, side)):
            c.start()

    def x_onward(b):
        for side in range(2):
            along_x(b, 0, side).wait_recv()
            along_x(b, 1, side).start()

    def z_hop(hop):
        for side in range(2):
            along_z(hop, side).wait_recv()
            if hop < NZ // 2:
                along_z(hop + 1, side).start()

    def dispatch(i):
        peer = plane_peer(ep, i)
        return remote(sent.at[peer], arrived.at[ep], a_send, a_recv, i, (peer, tp))

    def give_back(j, i):
        peer = plane_peer(ep, i)
        return remote(results.at[j, peer], returned.at[j, ep], r_send, r_recv, j * peers + i, (peer, tp))

    def each(first, last, act):
        def one(i, carry):
            act(i)
            return carry

        lax.fori_loop(first, last, one, 0)

    rows = rows_ref[...].astype(f32)
    squared = jnp.mean(rows * rows, axis=-1, keepdims=True)
    normed = (rows * lax.rsqrt(squared + EPS) * ffn_ref[...]).astype(jnp.bfloat16)
    sent[...] = jnp.dot(place_ref[...], normed, preferred_element_type=f32).astype(jnp.bfloat16).reshape(sent.shape)

    for c in keeps:
        c.wait()
    for c in swaps:
        c.wait()
    for c in both(lambda side: along_z(1, side)):
        c.start()
    x_first(0)
    each(1, 22, lambda i: dispatch(i).start())
    z_hop(1)
    x_first(1)
    x_first(2)
    each(22, 43, lambda i: dispatch(i).start())
    for side in range(2):
        gate_up(0, 0, side).wait_recv()
        gate_up(0, 2, side).start()
    z_hop(2)
    x_onward(0)
    x_first(3)
    x_first(4)
    each(43, 64, lambda i: dispatch(i).start())
    arrived[ep] = sent[ep]
    for side in range(2):
        gate_up(1, 0, side).wait_recv()
        gate_up(1, 2, side).start()
    for step in range(2):
        for c in both(lambda side: down(0, step, side)):
            c.start()
    for b in (1, 2):
        x_onward(b)
    z_hop(3)
    x_first(5)
    x_first(6)
    for b in (3, 4):
        x_onward(b)
    z_hop(4)
    x_first(7)

    scaled = queries[...] * jnp.bfloat16(0.125)
    column = lax.broadcasted_iota(jnp.int32, scaled.shape, 1)
    zero = jnp.zeros_like(scaled)
    spread[0 : 2 * count] = jnp.where(column < 64, scaled, zero)
    spread[2 * count :] = jnp.where(column < 64, zero, scaled)
    top[...] = jnp.full_like(top, -1e30)
    total[...] = jnp.zeros_like(total)
    acc[...] = jnp.zeros_like(acc)

    each(1, peers, lambda i: dispatch(i).wait_recv())
    for c in loads[:2]:
        c.wait()

    def one_part(s, carry):
        @pl.when(s == 1)
        def _():
            for n in range(2):
                gate_up(n, 1, 0).wait_recv()
            for b in (5, 6):
                x_onward(b)

        @pl.when(s == 2)
        def _():
            for n in range(2):
                gate_up(n, 1, 1).wait_recv()
            x_onward(7)

        @pl.when(s == 3)
        def _():
            for n in range(2):
                for side in range(2):
                    gate_up(n, 2, side).wait_recv()

        rows_in = arrived[...].reshape(peers * arrived.shape[1], arrived.shape[2])
        gate = jnp.dot(rows_in, gates[s], preferred_element_type=f32)
        up = jnp.dot(rows_in, ups[s], preferred_element_type=f32)
        hidden[:, pl.ds(pl.multiple_of(s * deep, deep), deep)] = (gate / (1.0 + jnp.exp(-gate)) * up).astype(jnp.bfloat16)
        return carry

    lax.fori_loop(0, NY, one_part, 0)

    def absorb(b, carry):
        at = pl.ds(pl.multiple_of(b * block, block), block)
        scores = lax.dot_general(spread[...], kv[at, 0:128], (((1,), (1,)), ((), ())), preferred_element_type=f32)
        old = top[...]
        new = jnp.maximum(old, jnp.max(scores, axis=-1, keepdims=True))
        factor = jnp.exp(old - new)
        weights = jnp.exp(scores - new)
        total[...] = total[...] * factor + jnp.sum(weights, axis=-1, keepdims=True)
        acc[...] = acc[...] * factor + jnp.dot(
            weights.astype(jnp.bfloat16), kv[at, 128:256], preferred_element_type=f32
        )
        top[...] = new
        return carry

    turns = kv.shape[0] // block

    def one_chunk(j, carry):
        for k in range(parts):
            @pl.when(j == k)
            def _(k=k):
                for side in range(2):
                    down(k, 0, side).wait_recv()
                    down(k, 2, side).start()
                if k + 1 < parts:
                    for step in range(2):
                        for c in both(lambda side: down(k + 1, step, side)):
                            c.start()
                loads[3 + k].wait()
                if k == 1:
                    for b in range(NZ):
                        for side in range(2):
                            along_x(b, 1, side).wait_recv()

        @pl.when(j > 0)
        def _():
            lax.fori_loop((j - 1) * turns // (parts - 1), j * turns // (parts - 1), absorb, 0)

        for k in range(parts):
            @pl.when(j == k)
            def _(k=k):
                for side in range(2):
                    down(k, 1, side).wait_recv()
                    down(k, 2, side).wait_recv()

        results[j] = (
            jnp.dot(hidden[...], downs[j], preferred_element_type=f32).astype(jnp.bfloat16).reshape(results.shape[1:])
        )
        returned[j, ep] = results[j, ep]
        each(1, peers, lambda i: give_back(j, i).start())
        return carry

    lax.fori_loop(0, parts, one_chunk, 0)

    per_head = acc[0 : 2 * count] / total[0 : 2 * count] - lam_ref[...] * (acc[2 * count :] / total[2 * count :])
    squared = jnp.mean(per_head * per_head, axis=-1, keepdims=True)
    normed = per_head * lax.rsqrt(squared + EPS) * gain_ref[...] * HEAD_SCALE
    done[...] = normed.astype(jnp.bfloat16).reshape(done.shape)

    def hand_on(i):
        to_core = lax.rem(core + i // NY, NC)
        to_tp = lax.rem(tp + i % NY, NY)
        return remote(
            done.at[to_core * NY + to_tp], heads.at[head], h_send, h_recv, i, (chip * NC + to_core, to_tp)
        )

    for i in range(1, NC * NY):
        hand_on(i).start()
    heads[head] = done[core * NY + tp]
    for i in range(1, NC * NY):
        hand_on(i).wait()
    loads[2].wait()
    attended = jnp.concatenate([heads[i] for i in range(NC * NY)], axis=1)
    mixer_ref[...] = jnp.dot(attended, w_out[...], preferred_element_type=f32).astype(jnp.bfloat16)

    def combine(j, carry):
        each(1, peers, lambda i: give_back(j, i).wait_recv())
        back = returned[j].reshape(peers * returned.shape[2], cols)
        moe_ref[:, pl.ds(pl.multiple_of(j * cols, cols), cols)] = (
            jnp.dot(high_ref[...], back, preferred_element_type=f32)
            + jnp.dot(low_ref[...], back, preferred_element_type=f32)
        ).astype(jnp.bfloat16)
        return carry

    lax.fori_loop(0, parts, combine, 0)

    each(1, peers, lambda i: dispatch(i).wait_send())
    for j in range(parts):
        each(1, peers, lambda i: give_back(j, i).wait_send())
    for side in range(2):
        for step in range(3):
            for n in range(2):
                gate_up(n, step, side).wait_send()
            for j in range(parts):
                down(j, step, side).wait_send()
        for hop in range(1, NZ // 2 + 1):
            along_z(hop, side).wait_send()
        for b in range(NZ):
            for step in range(2):
                along_x(b, step, side).wait_send()


def whole_step(parts, block, *args):
    q, k, v, lam, gain, w_out, rows, ffn, place, high, low, w_gate, w_up, w_down = args
    bf16, f32 = jnp.bfloat16, jnp.float32
    peers = NZ * NX * NC
    count, width = q.shape[0], rows.shape[1]
    capacity = place.shape[0] // peers
    deep = w_down.shape[0]
    own_rows = count // NY
    dma = lambda n: pltpu.SemaphoreType.DMA((n,))
    return pl.pallas_call(
        functools.partial(step_kernel, parts, block),
        name="whole_step",
        out_shape=(
            jax.ShapeDtypeStruct((own_rows, width), bf16),
            jax.ShapeDtypeStruct((rows.shape[0], width), bf16),
        ),
        in_specs=[ANY, ANY, ANY, VMEM, VMEM, ANY, VMEM, VMEM, VMEM, VMEM, VMEM, ANY, ANY, ANY],
        out_specs=(VMEM, VMEM),
        scratch_shapes=[
            pltpu.VMEM((NY, *w_gate.shape), bf16),
            pltpu.VMEM((NY, *w_up.shape), bf16),
            pltpu.VMEM((parts, NY * deep, width // parts), bf16),
            pltpu.VMEM((peers, capacity, width), bf16),
            pltpu.VMEM((peers, capacity, width), bf16),
            pltpu.VMEM((peers * capacity, NY * deep), bf16),
            pltpu.VMEM((parts, peers, capacity, width // parts), bf16),
            pltpu.VMEM((parts, peers, capacity, width // parts), bf16),
            pltpu.VMEM((2 * count, 128), bf16),
            pltpu.VMEM((4 * count, 128), bf16),
            pltpu.VMEM((peers * count, 256), bf16),
            pltpu.VMEM((4 * count, 1), f32),
            pltpu.VMEM((4 * count, 1), f32),
            pltpu.VMEM((4 * count, 128), f32),
            pltpu.VMEM((NC * NY, own_rows, 128), bf16),
            pltpu.VMEM((NC * NY, own_rows, 128), bf16),
            pltpu.VMEM(w_out.shape, bf16),
            dma(12), dma(12), dma(6 * parts), dma(6 * parts), dma(3), dma(3), dma(NZ), dma(NZ), dma(4 * NZ), dma(4 * NZ),
            dma(peers), dma(peers), dma(parts * peers), dma(parts * peers), dma(NC * NY), dma(NC * NY), dma(6 + parts),
        ],
        compiler_params=pltpu.CompilerParams(has_side_effects=True, vmem_limit_bytes=60 * 2**20),
        cost_estimate=pl.CostEstimate(flops=10**10, bytes_accessed=16 * 2**20, transcendentals=0),
    )(*args)


def local(
    query_rows, key_rows, value_rows, lambdas, head_gain, w_out, moe_rows, ffn_gain,
    routes, group_logits, pick_logits, w_gate, w_up, w_down,
):
    ep, tp = lax.axis_index("ep"), lax.axis_index("tp")
    core = ep % NC
    peers = NZ * NX * NC
    quarter = moe_rows.shape[0] // NY
    top_k = routes.shape[1]
    capacity = 8
    own = lambda a: lax.dynamic_slice_in_dim(a, tp * quarter, quarter, 0)
    picks = own(routes)
    flat = picks.reshape(-1)
    onehot = (flat[:, None] == jnp.arange(peers, dtype=jnp.int32)).astype(jnp.int32)
    ranking = jnp.sum((jnp.cumsum(onehot, axis=0) - onehot) * onehot, axis=-1)
    slots = (flat * capacity + ranking).reshape(quarter, top_k)
    every = jnp.arange(peers * capacity, dtype=jnp.int32)
    place = ((slots[None, :, 0] == every[:, None]) | (slots[None, :, 1] == every[:, None])).astype(jnp.bfloat16)
    group_count = group_logits.shape[1]
    group_prob = jax.nn.softmax(own(group_logits), axis=-1)
    matches = ((picks // (peers // group_count))[..., None] == jnp.arange(group_count, dtype=jnp.int32)).astype(
        jnp.float32
    )
    share = jnp.sum(group_prob[:, None, :] * matches, axis=-1)
    gate_values = share * jax.nn.softmax(own(pick_logits), axis=-1)
    mixing = jnp.sum(jnp.where(slots[:, :, None] == every, gate_values[:, :, None], 0.0), axis=1)
    high = mixing.astype(jnp.bfloat16)
    low = (mixing - high.astype(jnp.float32)).astype(jnp.bfloat16)
    return whole_step(
        4, 1024,
        query_rows, key_rows, value_rows, lax.dynamic_slice_in_dim(lambdas, core, 1, 0)[None], head_gain[None], w_out,
        own(moe_rows), ffn_gain[None], place, high, low, w_gate[0], w_up[0], w_down[0],
    )


def solution(mesh):
    return jax.shard_map(
        local,
        mesh=mesh,
        in_specs=(
            P("ep", "tp"), P("ep", "tp"), P("ep", "tp"), P("tp"), P(), P(), P("ep", None), P(), P("ep", None),
            P("ep", None), P("ep", None), P("ep", None, "tp"), P("ep", None, "tp"), P("ep", "tp", None),
        ),
        out_specs=(P(("ep", "tp"), None), P(("ep", "tp"), None)),
        check_vma=False,
    )
```

time: 228 us -> 192 us (0.84)
  Pallas kernels: 194 us -> 176 us
  between operations: 14.4 us -> 0.72 us
  matrix products: 7.11 us -> 0 us
  local copies, waits for them, and re-layouts: 3.82 us -> 7.51 us
  starting transfers between devices: 3.32 us -> 0 us
    pallas_call x3 -> x1, Pallas kernels: 194 us -> 176 us  [whole_step(): pl.pallas_call(functools.partial(step_kernel, parts, block), name='whole_...]
    dot_general x4 -> x0, matrix products: 7.11 us -> none  [the longest x1 2.18 us: local(): jnp.dot(high, back, preferred_element_type=jnp.float32)]
    ppermute x1 -> x0, starting transfers between devices: 3.29 us -> none  [local(): theirs = lax.ppermute(other, 'ep', [(i, i ^ 1) for i in range(peers)])]
    concatenate x3 -> x0, other arithmetic: 2.39 us -> none  [the longest x1 0.91 us: local(): jnp.concatenate([scaled[:, :64], zero], 1)]
  transfers between devices with their start and end apart: 2 -> 0, of which waited for: 1 -> 0; matrix products, arithmetic and copies ran while one was open for 3% -> 0% of each run, Pallas kernels for 56% -> 0%
where the time goes in v2:
time: 192 us; the launch traced here: 191 us
  Pallas kernels  176 us (92%)
  local copies, waits for them, and re-layouts  7.51 us (4%)
  other arithmetic  6.6 us (3%)
    pallas_call x1, Pallas kernels, whole_step(): pl.pallas_call(functools.partial(step_kernel, parts, block), name='whole_...  176 us

profile of v2, /device:TPU:1, one launch (start us, length us, event | category | flops | bytes accessed | tf_op | source)
XLA Modules:
  0.0 191.3 jit_solution(13031107343503191813)
XLA Ops:
  0.7 1.4 dynamic_slice.15
  2.1 0.7 dynamic-slice_reduce_fusion
  2.8 0.7 fusion.11
  3.5 0.7 fusion.10
  4.2 0.7 fusion.9
  4.9 0.7 fusion.8
  5.6 0.7 constant_dynamic-slice_fusion.1
  6.3 0.1 copy.32
  6.4 0.1 eq.87
  6.5 0.1 eq.83
  6.7 0.6 reduce-window.6
  7.3 0.2 slice_reduce_fusion.2
  7.5 0.1 fusion.5
  7.7 0.1 reduce_sum.48
  7.9 0.1 copy.31
  7.9 0.7 divide_multiply_fusion
  8.7 0.2 slice_reduce_fusion.1
  8.9 0.7 fusion.1.place_ref
  9.6 0.1 select_reduce_fusion
  9.8 0.7 subtract_convert_fusion
  10.5 0.8 constant_dynamic-slice_fusion.2.rows_ref
  11.3 176.5 %whole_step.1 = (bf16[48,2048]{1,0:T(8,128)(2,1)}, bf16[128,2048]{1,0:T(8,128)(2,1)}) custom-call(bf16[192,256]{1,0:T(8,128)(2,1)} %q_ref.1, bf16[192,256]{1,0:T(8,128)(2,1)} %k_ref.1, bf16[192,256]{1,0:T(8,128)(2,1)} %v_ref.1, f32[1,1]{1,0:T(1,128)} %bitcast.lam_ref, f32[1,128]{1,0:T(1,128)} %bitcast.29, bf16[1024,2048]{1,0:T(8,128)(2,1)} %w_out_ref.1, ...), custom_call_target="tpu_custom_call" | custom-call | flops 10000000000 | bytes 16777216 | tf_op jit(solution)/shard_map/whole_step/pallas_call | solution.py:355
  187.8 1.6 copy.37
  189.4 1.9 copy.38
  (8 shorter events, 0.2 us)
Async XLA Ops:
  0.6 9.9 %copy-start = (bf16[512,2048]{1,0:T(8,128)(2,1)S(1)}, bf16[512,2048]{1,0:T(8,128)(2,1)}, u32[]{:S(2)}) copy-start(bf16[512,2048]{1,0:T(8,128)(2,1)} %param.20) | copy-start | bytes 6291460

commit v3 on v2

--- a/solution.py
+++ b/solution.py
@@ -24,10 +24,10 @@
 
 
 def step_kernel(
-    parts, block,
-    q_ref, k_ref, v_ref, lam_ref, gain_ref, w_out_ref, rows_ref, ffn_ref, place_ref, high_ref, low_ref,
+    parts,
+    q_ref, k_ref, v_ref, lam_ref, gain_ref, w_out_ref, rows_ref, ffn_ref, routes_ref, groups_ref, picks_ref,
     g_ref, u_ref, d_ref, mixer_ref, moe_ref,
-    gates, ups, downs, sent, arrived, hidden, results, returned, queries, spread, kv, top, total, acc, done, heads, w_out,
+    rows_in, high, low, gates, ups, downs, sent, arrived, hidden, results, returned, queries, spread, kv, top, total, acc, done, heads, w_out,
     g_send, g_recv, d_send, d_recv, p_send, p_recv, z_send, z_recv, x_send, x_recv,
     a_send, a_recv, r_send, r_recv, h_send, h_recv, own_sem,
 ):
@@ -100,7 +100,11 @@
         pltpu.make_async_copy(d_ref.at[:, pl.ds(j * cols, cols)], downs.at[j, pl.ds(0, deep)], own_sem.at[6 + j])
         for j in range(parts)
     ]
-    for c in loads:
+    tokens = rows_in.shape[0]
+    load_rows = pltpu.make_async_copy(
+        rows_ref.at[pl.ds(pl.multiple_of(tp * tokens, tokens), tokens)], rows_in, own_sem.at[6 + parts]
+    )
+    for c in [load_rows] + loads:
         c.start()
 
     chip_rows = kv.shape[0] // (NZ * NX)
@@ -159,10 +163,45 @@
 
         lax.fori_loop(first, last, one, 0)
 
-    rows = rows_ref[...].astype(f32)
+    load_rows.wait()
+    rows = rows_in[...].astype(f32)
     squared = jnp.mean(rows * rows, axis=-1, keepdims=True)
     normed = (rows * lax.rsqrt(squared + EPS) * ffn_ref[...]).astype(jnp.bfloat16)
-    sent[...] = jnp.dot(place_ref[...], normed, preferred_element_type=f32).astype(jnp.bfloat16).reshape(sent.shape)
+    own_rows = pl.ds(pl.multiple_of(tp * tokens, tokens), tokens)
+    chosen = routes_ref[own_rows, :]
+    logits = groups_ref[own_rows, :]
+    group_weights = jnp.exp(logits - jnp.max(logits, axis=-1, keepdims=True))
+    group_weights = group_weights / jnp.sum(group_weights, axis=-1, keepdims=True)
+    logits = picks_ref[own_rows, :]
+    pick_weights = jnp.exp(logits - jnp.max(logits, axis=-1, keepdims=True))
+    pick_weights = pick_weights / jnp.sum(pick_weights, axis=-1, keepdims=True)
+    lane = lax.broadcasted_iota(jnp.int32, (tokens, tokens), 1)
+    earlier = (lane < lax.broadcasted_iota(jnp.int32, (tokens, tokens), 0)).astype(f32).astype(jnp.bfloat16)
+    named = [lane == chosen[:, k : k + 1] for k in range(2)]
+    either = jnp.where(named[0] | named[1], 1.0, 0.0).astype(jnp.bfloat16)
+    before = jnp.dot(earlier, either, preferred_element_type=f32)
+    capacity = sent.shape[1]
+    every = lax.broadcasted_iota(jnp.int32, (tokens, peers * capacity), 1).astype(f32)
+    group_size = peers // groups_ref.shape[1]
+    group_lane = lax.broadcasted_iota(jnp.int32, group_weights.shape, 1) * group_size
+    place = jnp.zeros((tokens, peers * capacity), f32)
+    mixing = jnp.zeros((tokens, peers * capacity), f32)
+    for k in range(2):
+        expert = chosen[:, k : k + 1]
+        rank = jnp.sum(jnp.where(named[k], before, 0.0), axis=-1, keepdims=True)
+        hit = every == expert.astype(f32) * capacity + rank
+        inside = (expert >= group_lane) & (expert < group_lane + group_size)
+        share = jnp.sum(jnp.where(inside, group_weights, 0.0), axis=-1, keepdims=True)
+        place = jnp.where(hit, 1.0, place)
+        mixing = jnp.where(hit, share * pick_weights[:, k : k + 1], mixing)
+    high[...] = mixing.astype(jnp.bfloat16)
+    low[...] = (mixing - mixing.astype(jnp.bfloat16).astype(f32)).astype(jnp.bfloat16)
+    sent[...] = (
+        lax.dot_general(place.astype(jnp.bfloat16), normed, (((0,), (0,)), ((), ())), preferred_element_type=f32)
+        .astype(jnp.bfloat16)
+        .reshape(sent.shape)
+    )
+    arrived[ep] = sent[ep]
 
     for c in keeps:
         c.wait()
@@ -171,35 +210,7 @@
     for c in both(lambda side: along_z(1, side)):
         c.start()
     x_first(0)
-    each(1, 22, lambda i: dispatch(i).start())
-    z_hop(1)
-    x_first(1)
-    x_first(2)
-    each(22, 43, lambda i: dispatch(i).start())
-    for side in range(2):
-        gate_up(0, 0, side).wait_recv()
-        gate_up(0, 2, side).start()
-    z_hop(2)
-    x_onward(0)
-    x_first(3)
-    x_first(4)
-    each(43, 64, lambda i: dispatch(i).start())
-    arrived[ep] = sent[ep]
-    for side in range(2):
-        gate_up(1, 0, side).wait_recv()
-        gate_up(1, 2, side).start()
-    for step in range(2):
-        for c in both(lambda side: down(0, step, side)):
-            c.start()
-    for b in (1, 2):
-        x_onward(b)
-    z_hop(3)
-    x_first(5)
-    x_first(6)
-    for b in (3, 4):
-        x_onward(b)
-    z_hop(4)
-    x_first(7)
+    each(1, peers, lambda i: dispatch(i).start())
 
     scaled = queries[...] * jnp.bfloat16(0.125)
     column = lax.broadcasted_iota(jnp.int32, scaled.shape, 1)
@@ -210,40 +221,29 @@
     total[...] = jnp.zeros_like(total)
     acc[...] = jnp.zeros_like(acc)
 
-    each(1, peers, lambda i: dispatch(i).wait_recv())
-    for c in loads[:2]:
-        c.wait()
-
-    def one_part(s, carry):
-        @pl.when(s == 1)
-        def _():
-            for n in range(2):
-                gate_up(n, 1, 0).wait_recv()
-            for b in (5, 6):
-                x_onward(b)
-
-        @pl.when(s == 2)
-        def _():
-            for n in range(2):
-                gate_up(n, 1, 1).wait_recv()
-            x_onward(7)
-
-        @pl.when(s == 3)
-        def _():
-            for n in range(2):
-                for side in range(2):
-                    gate_up(n, 2, side).wait_recv()
-
-        rows_in = arrived[...].reshape(peers * arrived.shape[1], arrived.shape[2])
-        gate = jnp.dot(rows_in, gates[s], preferred_element_type=f32)
-        up = jnp.dot(rows_in, ups[s], preferred_element_type=f32)
-        hidden[:, pl.ds(pl.multiple_of(s * deep, deep), deep)] = (gate / (1.0 + jnp.exp(-gate)) * up).astype(jnp.bfloat16)
-        return carry
-
-    lax.fori_loop(0, NY, one_part, 0)
-
-    def absorb(b, carry):
-        at = pl.ds(pl.multiple_of(b * block, block), block)
+    z_hop(1)
+    x_first(1)
+    x_first(2)
+    for n in range(2):
+        for side in range(2):
+            gate_up(n, 0, side).wait_recv()
+            gate_up(n, 2, side).start()
+    for j in range(2):
+        for step in range(2):
+            for c in both(lambda side: down(j, step, side)):
+                c.start()
+    x_onward(0)
+    for b in (1, 2):
+        x_onward(b)
+
+    def absorb(b):
+        for side in range(2):
+            along_x(b, 1, side).wait_recv()
+        size = NX * chip_rows
+        at = pl.ds(pl.multiple_of(at_z(blocks[b]) * size, size), size)
+        absorb_at(at)
+
+    def absorb_at(at):
         scores = lax.dot_general(spread[...], kv[at, 0:128], (((1,), (1,)), ((), ())), preferred_element_type=f32)
         old = top[...]
         new = jnp.maximum(old, jnp.max(scores, axis=-1, keepdims=True))
@@ -254,37 +254,82 @@
             weights.astype(jnp.bfloat16), kv[at, 128:256], preferred_element_type=f32
         )
         top[...] = new
+
+    for b in range(3):
+        absorb(b)
+
+    each(1, peers, lambda i: dispatch(i).wait_recv())
+    for c in loads[:2]:
+        c.wait()
+
+    def one_part(s, carry):
+        @pl.when(s == 1)
+        def _():
+            for n in range(2):
+                gate_up(n, 1, 0).wait_recv()
+            z_hop(2)
+            x_first(3)
+            x_first(4)
+
+        @pl.when(s == 2)
+        def _():
+            for n in range(2):
+                gate_up(n, 1, 1).wait_recv()
+
+        @pl.when(s == 3)
+        def _():
+            for n in range(2):
+                for side in range(2):
+                    gate_up(n, 2, side).wait_recv()
+
+        rows_at = arrived[...].reshape(peers * arrived.shape[1], arrived.shape[2])
+        gate = jnp.dot(rows_at, gates[s], preferred_element_type=f32)
+        up = jnp.dot(rows_at, ups[s], preferred_element_type=f32)
+        hidden[:, pl.ds(pl.multiple_of(s * deep, deep), deep)] = (gate / (1.0 + jnp.exp(-gate)) * up).astype(jnp.bfloat16)
         return carry
 
-    turns = kv.shape[0] // block
+    lax.fori_loop(0, NY, one_part, 0)
+
+    def down_onward(j):
+        for side in range(2):
+            down(j, 0, side).wait_recv()
+            down(j, 2, side).start()
+        if j + 2 < parts:
+            for step in range(2):
+                for c in both(lambda side: down(j + 2, step, side)):
+                    c.start()
+
+    def between(j):
+        if j == 0:
+            down_onward(0)
+            z_hop(3)
+            x_first(5)
+            x_first(6)
+            down_onward(1)
+            x_onward(3)
+            x_onward(4)
+            z_hop(4)
+            x_first(7)
+        elif j == 1:
+            down_onward(2)
+            x_onward(5)
+            x_onward(6)
+            absorb(3)
+            absorb(4)
+        elif j == 2:
+            down_onward(3)
+            x_onward(7)
+            absorb(5)
 
     def one_chunk(j, carry):
         for k in range(parts):
             @pl.when(j == k)
             def _(k=k):
-                for side in range(2):
-                    down(k, 0, side).wait_recv()
-                    down(k, 2, side).start()
-                if k + 1 < parts:
-                    for step in range(2):
-                        for c in both(lambda side: down(k + 1, step, side)):
-                            c.start()
-                loads[3 + k].wait()
-                if k == 1:
-                    for b in range(NZ):
-                        for side in range(2):
-                            along_x(b, 1, side).wait_recv()
-
-        @pl.when(j > 0)
-        def _():
-            lax.fori_loop((j - 1) * turns // (parts - 1), j * turns // (parts - 1), absorb, 0)
-
-        for k in range(parts):
-            @pl.when(j == k)
-            def _(k=k):
+                between(k)
                 for side in range(2):
                     down(k, 1, side).wait_recv()
                     down(k, 2, side).wait_recv()
+                loads[3 + k].wait()
 
         results[j] = (
             jnp.dot(hidden[...], downs[j], preferred_element_type=f32).astype(jnp.bfloat16).reshape(results.shape[1:])
@@ -294,6 +339,8 @@
         return carry
 
     lax.fori_loop(0, parts, one_chunk, 0)
+    absorb(6)
+    absorb(7)
 
     per_head = acc[0 : 2 * count] / total[0 : 2 * count] - lam_ref[...] * (acc[2 * count :] / total[2 * count :])
     squared = jnp.mean(per_head * per_head, axis=-1, keepdims=True)
@@ -320,8 +367,8 @@
         each(1, peers, lambda i: give_back(j, i).wait_recv())
         back = returned[j].reshape(peers * returned.shape[2], cols)
         moe_ref[:, pl.ds(pl.multiple_of(j * cols, cols), cols)] = (
-            jnp.dot(high_ref[...], back, preferred_element_type=f32)
-            + jnp.dot(low_ref[...], back, preferred_element_type=f32)
+            jnp.dot(high[...], back, preferred_element_type=f32)
+            + jnp.dot(low[...], back, preferred_element_type=f32)
         ).astype(jnp.bfloat16)
         return carry
 
@@ -343,25 +390,29 @@
                 along_x(b, step, side).wait_send()
 
 
-def whole_step(parts, block, *args):
-    q, k, v, lam, gain, w_out, rows, ffn, place, high, low, w_gate, w_up, w_down = args
+def whole_step(parts, *args):
+    q, k, v, lam, gain, w_out, rows, ffn, routes, groups, picks, w_gate, w_up, w_down = args
     bf16, f32 = jnp.bfloat16, jnp.float32
     peers = NZ * NX * NC
     count, width = q.shape[0], rows.shape[1]
-    capacity = place.shape[0] // peers
+    capacity = 8
+    tokens = rows.shape[0] // NY
     deep = w_down.shape[0]
     own_rows = count // NY
     dma = lambda n: pltpu.SemaphoreType.DMA((n,))
     return pl.pallas_call(
-        functools.partial(step_kernel, parts, block),
+        functools.partial(step_kernel, parts),
         name="whole_step",
         out_shape=(
             jax.ShapeDtypeStruct((own_rows, width), bf16),
-            jax.ShapeDtypeStruct((rows.shape[0], width), bf16),
+            jax.ShapeDtypeStruct((tokens, width), bf16),
         ),
-        in_specs=[ANY, ANY, ANY, VMEM, VMEM, ANY, VMEM, VMEM, VMEM, VMEM, VMEM, ANY, ANY, ANY],
+        in_specs=[ANY, ANY, ANY, VMEM, VMEM, ANY, ANY, VMEM, VMEM, VMEM, VMEM, ANY, ANY, ANY],
         out_specs=(VMEM, VMEM),
         scratch_shapes=[
+            pltpu.VMEM((tokens, width), bf16),
+            pltpu.VMEM((tokens, peers * capacity), bf16),
+            pltpu.VMEM((tokens, peers * capacity), bf16),
             pltpu.VMEM((NY, *w_gate.shape), bf16),
             pltpu.VMEM((NY, *w_up.shape), bf16),
             pltpu.VMEM((parts, NY * deep, width // parts), bf16),
@@ -380,7 +431,7 @@
             pltpu.VMEM((NC * NY, own_rows, 128), bf16),
             pltpu.VMEM(w_out.shape, bf16),
             dma(12), dma(12), dma(6 * parts), dma(6 * parts), dma(3), dma(3), dma(NZ), dma(NZ), dma(4 * NZ), dma(4 * NZ),
-            dma(peers), dma(peers), dma(parts * peers), dma(parts * peers), dma(NC * NY), dma(NC * NY), dma(6 + parts),
+            dma(peers), dma(peers), dma(parts * peers), dma(parts * peers), dma(NC * NY), dma(NC * NY), dma(7 + parts),
         ],
         compiler_params=pltpu.CompilerParams(has_side_effects=True, vmem_limit_bytes=60 * 2**20),
         cost_estimate=pl.CostEstimate(flops=10**10, bytes_accessed=16 * 2**20, transcendentals=0),
@@ -391,34 +442,11 @@
     query_rows, key_rows, value_rows, lambdas, head_gain, w_out, moe_rows, ffn_gain,
     routes, group_logits, pick_logits, w_gate, w_up, w_down,
 ):
-    ep, tp = lax.axis_index("ep"), lax.axis_index("tp")
-    core = ep % NC
-    peers = NZ * NX * NC
-    quarter = moe_rows.shape[0] // NY
-    top_k = routes.shape[1]
-    capacity = 8
-    own = lambda a: lax.dynamic_slice_in_dim(a, tp * quarter, quarter, 0)
-    picks = own(routes)
-    flat = picks.reshape(-1)
-    onehot = (flat[:, None] == jnp.arange(peers, dtype=jnp.int32)).astype(jnp.int32)
-    ranking = jnp.sum((jnp.cumsum(onehot, axis=0) - onehot) * onehot, axis=-1)
-    slots = (flat * capacity + ranking).reshape(quarter, top_k)
-    every = jnp.arange(peers * capacity, dtype=jnp.int32)
-    place = ((slots[None, :, 0] == every[:, None]) | (slots[None, :, 1] == every[:, None])).astype(jnp.bfloat16)
-    group_count = group_logits.shape[1]
-    group_prob = jax.nn.softmax(own(group_logits), axis=-1)
-    matches = ((picks // (peers // group_count))[..., None] == jnp.arange(group_count, dtype=jnp.int32)).astype(
-        jnp.float32
-    )
-    share = jnp.sum(group_prob[:, None, :] * matches, axis=-1)
-    gate_values = share * jax.nn.softmax(own(pick_logits), axis=-1)
-    mixing = jnp.sum(jnp.where(slots[:, :, None] == every, gate_values[:, :, None], 0.0), axis=1)
-    high = mixing.astype(jnp.bfloat16)
-    low = (mixing - high.astype(jnp.float32)).astype(jnp.bfloat16)
+    core = lax.axis_index("ep") % NC
     return whole_step(
-        4, 1024,
+        4,
         query_rows, key_rows, value_rows, lax.dynamic_slice_in_dim(lambdas, core, 1, 0)[None], head_gain[None], w_out,
-        own(moe_rows), ffn_gain[None], place, high, low, w_gate[0], w_up[0], w_down[0],
+        moe_rows, ffn_gain[None], routes, group_logits, pick_logits, w_gate[0], w_up[0], w_down[0],
     )
 
 

time: 192 us -> 175 us (0.911)
  Pallas kernels: 176 us -> 165 us
  other arithmetic: 6.6 us -> 0 us
    pallas_call x1, Pallas kernels: 176 us -> 165 us  [whole_step(): pl.pallas_call(functools.partial(step_kernel, parts), name='whole_step',...]
    unnamed x5, local copies, waits for them, and re-layouts: 3.62 us -> 8.12 us
where the time goes in v3:
time: 175 us
  Pallas kernels  165 us (94%)
  local copies, waits for them, and re-layouts  9.36 us (5%)
    pallas_call x1, Pallas kernels, whole_step(): pl.pallas_call(functools.partial(step_kernel, parts), name='whole_step',...  165 us
    unnamed x5, local copies, waits for them, and re-layouts  8.12 us

profile of v3, /device:TPU:1, one launch (start us, length us, event | category | flops | bytes accessed | tf_op | source)
XLA Modules:
  0.0 175.1 jit_solution(10702148783499288305)
XLA Ops:
  0.6 1.2 dynamic_slice.3
  1.9 1.5 copy.16.routes_ref
  3.4 1.5 copy.17.groups_ref
  5.0 1.5 copy.18.picks_ref
  6.5 165.1 %whole_step.1 = (bf16[48,2048]{1,0:T(8,128)(2,1)}, bf16[128,2048]{1,0:T(8,128)(2,1)}) custom-call(bf16[192,256]{1,0:T(8,128)(2,1)} %q_ref.1, bf16[192,256]{1,0:T(8,128)(2,1)} %k_ref.1, bf16[192,256]{1,0:T(8,128)(2,1)} %v_ref.1, f32[1,1]{1,0:T(1,128)} %bitcast.lam_ref, f32[1,128]{1,0:T(1,128)} %bitcast.10, bf16[1024,2048]{1,0:T(8,128)(2,1)} %w_out_ref.1, ...), custom_call_target="tpu_custom_call" | custom-call | flops 10000000000 | bytes 16777216 | tf_op jit(solution)/shard_map/whole_step/pallas_call | solution.py:403
  171.6 1.6 copy.21
  173.2 1.9 %copy.22 = bf16[128,2048]{1,0:T(8,128)(2,1)} copy(bf16[128,2048]{1,0:T(8,128)(2,1)} %get-tuple-element.5) | data formatting | bytes 1048576

commit v4 on v3

--- a/solution.py
+++ b/solution.py
@@ -1,5 +1,3 @@
-import functools
-
 import jax
 import jax.numpy as jnp
 from jax import lax
@@ -9,6 +7,7 @@
 
 EPS = 1e-06
 HEAD_SCALE = 0.8
+PIECES = (256, 512, 640, 640)
 NZ, NX, NC, NY = 8, 4, 2, 4
 ANY = pl.BlockSpec(memory_space=pl.ANY)
 VMEM = pl.BlockSpec(memory_space=pltpu.VMEM)
@@ -24,13 +23,15 @@
 
 
 def step_kernel(
-    parts,
     q_ref, k_ref, v_ref, lam_ref, gain_ref, w_out_ref, rows_ref, ffn_ref, routes_ref, groups_ref, picks_ref,
     g_ref, u_ref, d_ref, mixer_ref, moe_ref,
-    rows_in, high, low, gates, ups, downs, sent, arrived, hidden, results, returned, queries, spread, kv, top, total, acc, done, heads, w_out,
+    rows_in, high, low, gates, ups, sent, arrived, hidden, queries, spread, kv, top, total, acc, done, heads, w_out,
     g_send, g_recv, d_send, d_recv, p_send, p_recv, z_send, z_recv, x_send, x_recv,
-    a_send, a_recv, r_send, r_recv, h_send, h_recv, own_sem,
+    a_send, a_recv, r_send, r_recv, h_send, h_recv, own_sem, met, *pieces,
 ):
+    parts = len(PIECES)
+    starts = [sum(PIECES[:j]) for j in range(parts)]
+    downs, results, returned = pieces[:parts], pieces[parts : 2 * parts], pieces[2 * parts :]
     ep, tp = lax.axis_index("ep"), lax.axis_index("tp")
     z, x, core = ep // (NX * NC), ep // NC % NX, ep % NC
     chip = ep // NC
@@ -56,19 +57,44 @@
         return remote(frm, to, g_send, g_recv, (n * 3 + step) * 2 + side, (ep, tp_side[side]))
 
     def down(j, step, side):
-        cols = downs.shape[2]
         rows = d_ref.shape[0] // 2
         h = (step + side) % 2 if step < 2 else side
         row = lambda place: pl.ds((place * 2 + h) * rows, rows)
         if step < 2:
-            frm = d_ref.at[pl.ds(h * rows, rows), pl.ds(j * cols, cols)]
-            to = downs.at[j, row(1 + side)]
+            frm = d_ref.at[pl.ds(h * rows, rows), pl.ds(starts[j], PIECES[j])]
+            to = downs[j].at[row(1 + side)]
         else:
-            frm = downs.at[j, row(1 + side)]
-            to = downs.at[j, row(3)]
+            frm = downs[j].at[row(1 + side)]
+            to = downs[j].at[row(3)]
         return remote(frm, to, d_send, d_recv, (j * 3 + step) * 2 + side, (ep, tp_side[side]))
 
     both = lambda make: [make(0), make(1)]
+
+    def down_first(j):
+        for step in range(2):
+            for c in both(lambda side: down(j, step, side)):
+                c.start()
+
+    def down_onward(j):
+        for side in range(2):
+            down(j, 0, side).wait_recv()
+            down(j, 2, side).start()
+
+    partner = chip * NC + 1 - core
+    next_z = [((lax.rem(z + dz, NZ) * NX + x) * NC + core, tp) for dz in (1, NZ - 1)]
+    next_x = [((z * NX + lax.rem(x + dx, NX)) * NC + core, tp) for dx in (1, NX - 1)]
+    next_y = [(ep, side) for side in tp_side]
+    near = next_z + next_x + next_y + [(partner, tp)]
+    barrier = pltpu.get_barrier_semaphore()
+    for device in near:
+        pl.semaphore_signal(barrier, inc=1, device_id=device, device_id_type=MESH)
+    pl.semaphore_wait(barrier, len(near))
+
+    def meet(turn, devices):
+        for n, device in enumerate(devices):
+            pl.semaphore_signal(met.at[turn * 2 + n], inc=1, device_id=device, device_id_type=MESH)
+        for n in range(len(devices)):
+            pl.semaphore_wait(met.at[turn * 2 + n], 1)
 
     for step in range(2):
         for n in range(2):
@@ -85,19 +111,17 @@
         (k_ref, kv.at[kv_rows, pl.ds(0, 128)]),
         (v_ref, kv.at[kv_rows, pl.ds(128, 128)]),
     )
-    partner = chip * NC + 1 - core
     swaps = [remote(src.at[:, other], dst, p_send, p_recv, n, (partner, tp)) for n, (src, dst) in enumerate(triples)]
     keeps = [pltpu.make_async_copy(src.at[:, mine], dst, own_sem.at[n]) for n, (src, dst) in enumerate(triples)]
     for c in swaps + keeps:
         c.start()
     deep = d_ref.shape[0]
-    cols = downs.shape[2]
     loads = [
         pltpu.make_async_copy(g_ref, gates.at[0], own_sem.at[3]),
         pltpu.make_async_copy(u_ref, ups.at[0], own_sem.at[4]),
         pltpu.make_async_copy(w_out_ref, w_out, own_sem.at[5]),
     ] + [
-        pltpu.make_async_copy(d_ref.at[:, pl.ds(j * cols, cols)], downs.at[j, pl.ds(0, deep)], own_sem.at[6 + j])
+        pltpu.make_async_copy(d_ref.at[:, pl.ds(starts[j], PIECES[j])], downs[j].at[pl.ds(0, deep)], own_sem.at[6 + j])
         for j in range(parts)
     ]
     tokens = rows_in.shape[0]
@@ -154,7 +178,7 @@
 
     def give_back(j, i):
         peer = plane_peer(ep, i)
-        return remote(results.at[j, peer], returned.at[j, ep], r_send, r_recv, j * peers + i, (peer, tp))
+        return remote(results[j].at[peer], returned[j].at[ep], r_send, r_recv, j * peers + i, (peer, tp))
 
     def each(first, last, act):
         def one(i, carry):
@@ -168,21 +192,30 @@
     squared = jnp.mean(rows * rows, axis=-1, keepdims=True)
     normed = (rows * lax.rsqrt(squared + EPS) * ffn_ref[...]).astype(jnp.bfloat16)
     own_rows = pl.ds(pl.multiple_of(tp * tokens, tokens), tokens)
-    chosen = routes_ref[own_rows, :]
-    logits = groups_ref[own_rows, :]
+    lane = lax.broadcasted_iota(jnp.int32, (tokens, tokens), 1)
+    below = lax.broadcasted_iota(jnp.int32, (tokens, tokens), 0)
+
+    def columns(ref):
+        rows = ref[:, own_rows].astype(f32)
+        turned = [
+            jnp.sum(jnp.where(lane == below, rows[k : k + 1], 0.0), axis=-1, keepdims=True) for k in range(ref.shape[0])
+        ]
+        return jnp.concatenate(turned, axis=1)
+
+    chosen = columns(routes_ref).astype(jnp.int32)
+    logits = columns(groups_ref)
     group_weights = jnp.exp(logits - jnp.max(logits, axis=-1, keepdims=True))
     group_weights = group_weights / jnp.sum(group_weights, axis=-1, keepdims=True)
-    logits = picks_ref[own_rows, :]
+    logits = columns(picks_ref)
     pick_weights = jnp.exp(logits - jnp.max(logits, axis=-1, keepdims=True))
     pick_weights = pick_weights / jnp.sum(pick_weights, axis=-1, keepdims=True)
-    lane = lax.broadcasted_iota(jnp.int32, (tokens, tokens), 1)
-    earlier = (lane < lax.broadcasted_iota(jnp.int32, (tokens, tokens), 0)).astype(f32).astype(jnp.bfloat16)
+    earlier = (lane < below).astype(f32).astype(jnp.bfloat16)
     named = [lane == chosen[:, k : k + 1] for k in range(2)]
     either = jnp.where(named[0] | named[1], 1.0, 0.0).astype(jnp.bfloat16)
     before = jnp.dot(earlier, either, preferred_element_type=f32)
     capacity = sent.shape[1]
     every = lax.broadcasted_iota(jnp.int32, (tokens, peers * capacity), 1).astype(f32)
-    group_size = peers // groups_ref.shape[1]
+    group_size = peers // groups_ref.shape[0]
     group_lane = lax.broadcasted_iota(jnp.int32, group_weights.shape, 1) * group_size
     place = jnp.zeros((tokens, peers * capacity), f32)
     mixing = jnp.zeros((tokens, peers * capacity), f32)
@@ -210,6 +243,11 @@
     for c in both(lambda side: along_z(1, side)):
         c.start()
     x_first(0)
+    for turn in range(3):
+        meet(turn, next_z)
+    for turn in range(3, 5):
+        meet(turn, next_x)
+    meet(5, [(partner, tp)])
     each(1, peers, lambda i: dispatch(i).start())
 
     scaled = queries[...] * jnp.bfloat16(0.125)
@@ -224,24 +262,28 @@
     z_hop(1)
     x_first(1)
     x_first(2)
-    for n in range(2):
-        for side in range(2):
-            gate_up(n, 0, side).wait_recv()
-            gate_up(n, 2, side).start()
-    for j in range(2):
-        for step in range(2):
-            for c in both(lambda side: down(j, step, side)):
-                c.start()
-    x_onward(0)
-    for b in (1, 2):
+    for side in range(2):
+        gate_up(0, 0, side).wait_recv()
+        gate_up(0, 2, side).start()
+    down_first(0)
+    for side in range(2):
+        gate_up(1, 0, side).wait_recv()
+        gate_up(1, 2, side).start()
+    for b in range(3):
         x_onward(b)
 
-    def absorb(b):
-        for side in range(2):
-            along_x(b, 1, side).wait_recv()
+    def absorb(first, last):
         size = NX * chip_rows
-        at = pl.ds(pl.multiple_of(at_z(blocks[b]) * size, size), size)
-        absorb_at(at)
+
+        def one(b, carry):
+            for side in range(2):
+                half = kv.at[pl.ds(0, chip_rows // 2)]
+                remote(half, half, x_send, x_recv, (b * 2 + 1) * 2 + side, (partner, tp)).wait_recv()
+            dz = jnp.where(b % 2 == 1, NZ - (b + 1) // 2, b // 2)
+            absorb_at(pl.ds(pl.multiple_of(lax.rem(z + dz, NZ) * size, size), size))
+            return carry
+
+        lax.fori_loop(first, last, one, 0)
 
     def absorb_at(at):
         scores = lax.dot_general(spread[...], kv[at, 0:128], (((1,), (1,)), ((), ())), preferred_element_type=f32)
@@ -255,8 +297,9 @@
         )
         top[...] = new
 
-    for b in range(3):
-        absorb(b)
+    for turn in range(6, 8):
+        meet(turn, next_y)
+    absorb(0, 3)
 
     each(1, peers, lambda i: dispatch(i).wait_recv())
     for c in loads[:2]:
@@ -290,59 +333,48 @@
 
     lax.fori_loop(0, NY, one_part, 0)
 
-    def down_onward(j):
-        for side in range(2):
-            down(j, 0, side).wait_recv()
-            down(j, 2, side).start()
-        if j + 2 < parts:
-            for step in range(2):
-                for c in both(lambda side: down(j + 2, step, side)):
-                    c.start()
-
     def between(j):
         if j == 0:
             down_onward(0)
+            down_first(1)
             z_hop(3)
             x_first(5)
             x_first(6)
+        elif j == 1:
             down_onward(1)
+            down_first(2)
             x_onward(3)
             x_onward(4)
             z_hop(4)
             x_first(7)
-        elif j == 1:
+        elif j == 2:
             down_onward(2)
+            down_first(3)
             x_onward(5)
             x_onward(6)
-            absorb(3)
-            absorb(4)
-        elif j == 2:
+            absorb(3, 4)
+        elif j == 3:
             down_onward(3)
             x_onward(7)
-            absorb(5)
-
-    def one_chunk(j, carry):
-        for k in range(parts):
-            @pl.when(j == k)
-            def _(k=k):
-                between(k)
-                for side in range(2):
-                    down(k, 1, side).wait_recv()
-                    down(k, 2, side).wait_recv()
-                loads[3 + k].wait()
-
-        results[j] = (
-            jnp.dot(hidden[...], downs[j], preferred_element_type=f32).astype(jnp.bfloat16).reshape(results.shape[1:])
+            absorb(4, 5)
+
+    for j in range(parts):
+        between(j)
+        for side in range(2):
+            down(j, 1, side).wait_recv()
+            down(j, 2, side).wait_recv()
+        loads[3 + j].wait()
+        results[j][...] = (
+            jnp.dot(hidden[...], downs[j][...], preferred_element_type=f32)
+            .astype(jnp.bfloat16)
+            .reshape(results[j].shape)
         )
-        returned[j, ep] = results[j, ep]
+        returned[j][ep] = results[j][ep]
         each(1, peers, lambda i: give_back(j, i).start())
-        return carry
-
-    lax.fori_loop(0, parts, one_chunk, 0)
-    absorb(6)
-    absorb(7)
-
-    per_head = acc[0 : 2 * count] / total[0 : 2 * count] - lam_ref[...] * (acc[2 * count :] / total[2 * count :])
+    absorb(5, 8)
+
+    lam = jnp.where(core == 0, lam_ref[:, 0:1], lam_ref[:, 1:2])
+    per_head = acc[0 : 2 * count] / total[0 : 2 * count] - lam * (acc[2 * count :] / total[2 * count :])
     squared = jnp.mean(per_head * per_head, axis=-1, keepdims=True)
     normed = per_head * lax.rsqrt(squared + EPS) * gain_ref[...] * HEAD_SCALE
     done[...] = normed.astype(jnp.bfloat16).reshape(done.shape)
@@ -363,16 +395,12 @@
     attended = jnp.concatenate([heads[i] for i in range(NC * NY)], axis=1)
     mixer_ref[...] = jnp.dot(attended, w_out[...], preferred_element_type=f32).astype(jnp.bfloat16)
 
-    def combine(j, carry):
+    for j in range(parts):
         each(1, peers, lambda i: give_back(j, i).wait_recv())
-        back = returned[j].reshape(peers * returned.shape[2], cols)
-        moe_ref[:, pl.ds(pl.multiple_of(j * cols, cols), cols)] = (
-            jnp.dot(high[...], back, preferred_element_type=f32)
-            + jnp.dot(low[...], back, preferred_element_type=f32)
+        back = returned[j][...].reshape(peers * capacity, PIECES[j])
+        moe_ref[:, starts[j] : starts[j] + PIECES[j]] = (
+            jnp.dot(high[...], back, preferred_element_type=f32) + jnp.dot(low[...], back, preferred_element_type=f32)
         ).astype(jnp.bfloat16)
-        return carry
-
-    lax.fori_loop(0, parts, combine, 0)
 
     each(1, peers, lambda i: dispatch(i).wait_send())
     for j in range(parts):
@@ -390,7 +418,7 @@
                 along_x(b, step, side).wait_send()
 
 
-def whole_step(parts, *args):
+def whole_step(*args):
     q, k, v, lam, gain, w_out, rows, ffn, routes, groups, picks, w_gate, w_up, w_down = args
     bf16, f32 = jnp.bfloat16, jnp.float32
     peers = NZ * NX * NC
@@ -399,9 +427,10 @@
     tokens = rows.shape[0] // NY
     deep = w_down.shape[0]
     own_rows = count // NY
+    parts = len(PIECES)
     dma = lambda n: pltpu.SemaphoreType.DMA((n,))
     return pl.pallas_call(
-        functools.partial(step_kernel, parts),
+        step_kernel,
         name="whole_step",
         out_shape=(
             jax.ShapeDtypeStruct((own_rows, width), bf16),
@@ -415,12 +444,9 @@
             pltpu.VMEM((tokens, peers * capacity), bf16),
             pltpu.VMEM((NY, *w_gate.shape), bf16),
             pltpu.VMEM((NY, *w_up.shape), bf16),
-            pltpu.VMEM((parts, NY * deep, width // parts), bf16),
             pltpu.VMEM((peers, capacity, width), bf16),
             pltpu.VMEM((peers, capacity, width), bf16),
             pltpu.VMEM((peers * capacity, NY * deep), bf16),
-            pltpu.VMEM((parts, peers, capacity, width // parts), bf16),
-            pltpu.VMEM((parts, peers, capacity, width // parts), bf16),
             pltpu.VMEM((2 * count, 128), bf16),
             pltpu.VMEM((4 * count, 128), bf16),
             pltpu.VMEM((peers * count, 256), bf16),
@@ -432,8 +458,11 @@
             pltpu.VMEM(w_out.shape, bf16),
             dma(12), dma(12), dma(6 * parts), dma(6 * parts), dma(3), dma(3), dma(NZ), dma(NZ), dma(4 * NZ), dma(4 * NZ),
             dma(peers), dma(peers), dma(parts * peers), dma(parts * peers), dma(NC * NY), dma(NC * NY), dma(7 + parts),
-        ],
-        compiler_params=pltpu.CompilerParams(has_side_effects=True, vmem_limit_bytes=60 * 2**20),
+            pltpu.SemaphoreType.REGULAR((16,)),
+        ]
+        + [pltpu.VMEM((NY * deep, cols), bf16) for cols in PIECES]
+        + [pltpu.VMEM((peers, capacity, cols), bf16) for cols in PIECES * 2],
+        compiler_params=pltpu.CompilerParams(collective_id=0, has_side_effects=True, vmem_limit_bytes=60 * 2**20),
         cost_estimate=pl.CostEstimate(flops=10**10, bytes_accessed=16 * 2**20, transcendentals=0),
     )(*args)
 
@@ -442,11 +471,9 @@
     query_rows, key_rows, value_rows, lambdas, head_gain, w_out, moe_rows, ffn_gain,
     routes, group_logits, pick_logits, w_gate, w_up, w_down,
 ):
-    core = lax.axis_index("ep") % NC
     return whole_step(
-        4,
-        query_rows, key_rows, value_rows, lax.dynamic_slice_in_dim(lambdas, core, 1, 0)[None], head_gain[None], w_out,
-        moe_rows, ffn_gain[None], routes, group_logits, pick_logits, w_gate[0], w_up[0], w_down[0],
+        query_rows, key_rows, value_rows, lambdas[None], head_gain[None], w_out,
+        moe_rows, ffn_gain[None], routes.T, group_logits.T, pick_logits.T, w_gate[0], w_up[0], w_down[0],
     )
 
 

time: 175 us -> 153 us (0.87)
  Pallas kernels: 165 us -> 149 us
  local copies, waits for them, and re-layouts: 9.36 us -> 3.5 us
    pallas_call x1, Pallas kernels: 165 us -> 149 us  [whole_step(): pl.pallas_call(step_kernel, name='whole_step', out_shape=(jax.ShapeDtypeS...]
    unnamed x5 -> x2, local copies, waits for them, and re-layouts: 8.12 us -> 3.5 us
where the time goes in v4:
time: 153 us
  Pallas kernels  149 us (97%)
  local copies, waits for them, and re-layouts  3.5 us (2%)
    pallas_call x1, Pallas kernels, whole_step(): pl.pallas_call(step_kernel, name='whole_step', out_shape=(jax.ShapeDtypeS...  149 us
    unnamed x2, local copies, waits for them, and re-layouts  3.5 us

profile of v4, /device:TPU:1, one launch (start us, length us, event | category | flops | bytes accessed | tf_op | source)
XLA Modules:
  0.0 152.8 jit_solution(16047816129917358112)
XLA Ops:
  0.6 148.7 %whole_step.1 = (bf16[48,2048]{1,0:T(8,128)(2,1)}, bf16[128,2048]{1,0:T(8,128)(2,1)}) custom-call(bf16[192,256]{1,0:T(8,128)(2,1)} %q_ref.1, bf16[192,256]{1,0:T(8,128)(2,1)} %k_ref.1, bf16[192,256]{1,0:T(8,128)(2,1)} %v_ref.1, f32[1,2]{1,0:T(1,128)} %bitcast.16, f32[1,128]{1,0:T(1,128)} %bitcast.17, bf16[1024,2048]{1,0:T(8,128)(2,1)} %w_out_ref.1, ...), custom_call_target="tpu_custom_call" | custom-call | flops 10000000000 | bytes 16777216 | tf_op jit(solution)/shard_map/whole_step/pallas_call | solution.py:432
  149.3 1.6 %copy.18 = bf16[48,2048]{1,0:T(8,128)(2,1)} copy(bf16[48,2048]{1,0:T(8,128)(2,1)} %get-tuple-element.4) | data formatting | bytes 393216
  150.9 1.9 %copy.19 = bf16[128,2048]{1,0:T(8,128)(2,1)} copy(bf16[128,2048]{1,0:T(8,128)(2,1)} %get-tuple-element.5) | data formatting | bytes 1048576
